TPU v7x, 128 devices: a whole 4x4x4 slice. The times are simulated.
128 devices in a mesh: sp: 32 (over z, y, core), tp: 4 (over x).
Axes of the slice: x: 4, y: 4, z: 4, core: 2. Of those that a mesh axis runs over, the one named last changes fastest.
Arguments:
- resid_in: bfloat16 [12288, 2048], P('sp'), may hold values from -6 to 6
- cotangent: bfloat16 [12288, 2048], P('sp'), may hold values from -2 to 2
- norm_gain: float32 [2048], replicated, may hold values from 0.1 to 1.9
- routes: int32 [12288, 2], P('sp'), may hold values from 0 to 31, all different within a row; in each aligned block of 384 rows (0 to 383, 384 to 767, ...) at most 48 rows name the same one
- route_weights: float32 [12288, 2], P('sp'), may hold values from 0.1 to 1
- gate_weight: bfloat16 [32, 2048, 1024], P('sp', None, 'tp'), may hold values from -0.125 to 0.125
- up_weight: bfloat16 [32, 2048, 1024], P('sp', None, 'tp'), may hold values from -0.125 to 0.125
- down_weight: bfloat16 [32, 1024, 2048], P('sp', 'tp'), may hold values from -0.1875 to 0.1875
- out_weight: bfloat16 [2048, 1024], P(None, 'tp'), may hold values from -0.1875 to 0.1875
- gate_b: bfloat16 [12288, 1024], P('sp', 'tp'), may hold values from -6 to 6
- gate_c: bfloat16 [12288, 1024], P('sp', 'tp'), may hold values from -6 to 6
- values_u: bfloat16 [12288, 1024], P('sp', 'tp'), may hold values from -6 to 6
- taps: float32 [3, 1024], P(None, 'tp'), may hold values from -3.5 to 3.5
Outputs:
- grad_gate_weight: float32 [32, 2048, 1024], P('sp', None, 'tp')
- grad_up_weight: float32 [32, 2048, 1024], P('sp', None, 'tp')
- grad_down_weight: float32 [32, 1024, 2048], P('sp', 'tp')
- grad_resid: bfloat16 [12288, 2048], P('sp')
- grad_out_weight: float32 [2048, 1024], P('sp', 'tp')
- grad_gate_b: bfloat16 [12288, 1024], P('sp', 'tp')
- grad_gate_c: bfloat16 [12288, 1024], P('sp', 'tp')
- grad_values: bfloat16 [12288, 1024], P('sp', 'tp')
Inputs may be any that keep to these rules, and one draw needn't show every extreme that they name: `routes`: A row's 2 experts differ. In the rows of one index of sp (384 tokens) no expert is named more than 48 times, a bound that some block reaches.
All inputs are finite; a program needn't handle non-finite values.
Results may differ from a plain program's by a relative error of at most 0.024.
Values may be sent and summed in bfloat16 or wider, within the bound.
A program may use at most 128 MiB of HBM per device.

v0:
```python
import jax
import jax.numpy as jnp
from jax import lax
from jax.experimental import pallas as pl
from jax.experimental.pallas import tpu as pltpu
from jax.sharding import PartitionSpec as P

norm_eps = 1e-06


def passed_along(array, axis, by):
    size = lax.axis_size(axis)
    pairs = [(i, i + by) for i in range(size) if 0 <= i + by < size]
    return lax.ppermute(array, axis, pairs)


def cut_along(array, dim, size):
    before, after = (array.shape[:dim], array.shape[dim + 1 :])
    return jnp.moveaxis(array.reshape(*before, size, -1, *after), dim, 0)


def sum_at_owner(array, axis, dim):
    size = lax.axis_size(axis)
    tiles = lax.all_to_all(cut_along(array, dim, size), axis, 0, 0, tiled=True)
    return jnp.sum(tiles.astype(jnp.float32), axis=0)


MESH = pl.DeviceIdType.MESH
BF16 = jnp.bfloat16
F32 = jnp.float32
SLOTS = 48


def offsets(k):
    m = 7 * k
    return (m // 8) % 4, (m // 2) % 4, m % 2


def moved(s, k, sign):
    z, y, c = s // 8, (s // 2) % 4, s % 2
    dz, dy, dc = offsets(k)
    z = lax.rem(z + 4 + sign * dz, 4)
    y = lax.rem(y + 4 + sign * dy, 4)
    return (z * 4 + y) * 2 + lax.rem(c + dc, 2)


def greet_all(s, x, near):
    barrier = pltpu.get_barrier_semaphore()

    def greet(k, carry):
        pl.semaphore_signal(
            barrier, inc=1, device_id={"sp": moved(s, k, 1), "tp": x}, device_id_type=MESH
        )
        return carry

    lax.fori_loop(1, 32, greet, 0)
    for lane in near:
        pl.semaphore_signal(barrier, inc=1, device_id={"sp": s, "tp": lane}, device_id_type=MESH)
    pl.semaphore_wait(barrier, 31 + len(near))


def dispatch_kernel(packed, both, far_send, far_recv, near_send, near_recv, own_sem):
    s, x = lax.axis_index("sp"), lax.axis_index("tp")
    kind = lax.rem(x, 2)
    half = packed.shape[2] // 2
    sides = (lax.rem(x + 1, 4), lax.rem(x + 3, 4))
    greet_all(s, x, sides)

    def far(k):
        peer = moved(s, k, 1)
        return pltpu.make_async_remote_copy(
            src_ref=packed.at[peer],
            dst_ref=both.at[kind, s],
            send_sem=far_send.at[k],
            recv_sem=far_recv.at[k],
            device_id={"sp": peer, "tp": x},
            device_id_type=MESH,
        )

    def near(h, k, own=False):
        source = s if own else moved(s, k, -1)
        cols = pl.ds(h * half, half)
        return pltpu.make_async_remote_copy(
            src_ref=packed.at[source, :, cols] if own else both.at[kind, source, :, cols],
            dst_ref=both.at[kind, source, :, cols],
            send_sem=near_send.at[h, k],
            recv_sem=near_recv.at[h, k],
            device_id={"sp": s, "tp": sides[h]},
            device_id_type=MESH,
        )

    keep = pltpu.make_async_copy(packed.at[s], both.at[kind, s], own_sem)

    def go(k, carry):
        far(k).start()
        return carry

    lax.fori_loop(1, 32, go, 0)
    keep.start()
    for h in range(2):
        near(h, 0, True).start()

    def forward(k, carry):
        far(k).wait_recv()
        for h in range(2):
            near(h, k).start()
        return carry

    lax.fori_loop(1, 32, forward, 0)
    keep.wait()
    for h in range(2):
        near(h, 0, True).wait()

    def finish(k, carry):
        far(k).wait_send()
        for h in range(2):
            near(h, k).wait()
        return carry

    lax.fori_loop(1, 32, finish, 0)


def dispatch(packed):
    spec = pl.BlockSpec(memory_space=pl.ANY)
    return pl.pallas_call(
        dispatch_kernel,
        out_shape=jax.ShapeDtypeStruct((2,) + packed.shape, BF16),
        in_specs=[spec],
        out_specs=spec,
        scratch_shapes=[
            pltpu.SemaphoreType.DMA((32,)),
            pltpu.SemaphoreType.DMA((32,)),
            pltpu.SemaphoreType.DMA((2, 32)),
            pltpu.SemaphoreType.DMA((2, 32)),
            pltpu.SemaphoreType.DMA,
        ],
        compiler_params=pltpu.CompilerParams(collective_id=0, has_side_effects=True),
    )(packed)


def expert_pass(entry_rows, entry_cots, gate_mat, up_mat, down_mat):
    f32 = jnp.float32
    bf16 = jnp.bfloat16
    gate_pre = jnp.dot(entry_rows, gate_mat, preferred_element_type=f32)
    up_pre = jnp.dot(entry_rows, up_mat, preferred_element_type=f32)
    logistic = jax.nn.sigmoid(gate_pre)
    activated = gate_pre * logistic
    hidden = (activated * up_pre).astype(bf16)
    grad_down = jnp.einsum("rf,rd->fd", hidden, entry_cots, preferred_element_type=f32)
    dhidden = jnp.einsum("rd,fd->rf", entry_cots, down_mat, preferred_element_type=f32)
    dgate = (dhidden * up_pre * logistic * (1.0 + gate_pre * (1.0 - logistic))).astype(bf16)
    dup = (dhidden * activated).astype(bf16)
    grad_gate = jnp.einsum("rd,rf->df", entry_rows, dgate, preferred_element_type=f32)
    grad_up = jnp.einsum("rd,rf->df", entry_rows, dup, preferred_element_type=f32)
    partial_sum = jnp.einsum("rf,df->rd", dgate, gate_mat, preferred_element_type=f32) + jnp.einsum(
        "rf,df->rd", dup, up_mat, preferred_element_type=f32
    )
    return (grad_gate, grad_up, grad_down, partial_sum)


def on_device(
    resid_in,
    cotangent,
    norm_gain,
    routes,
    route_weights,
    gate_weight,
    up_weight,
    down_weight,
    out_weight,
    gate_b,
    gate_c,
    values_u,
    taps,
):
    f32 = jnp.float32
    bf16 = jnp.bfloat16
    token_count, model_width = resid_in.shape
    groups = lax.axis_size("sp")
    lanes = lax.axis_size("tp")
    local_experts = gate_weight.shape[0]
    expert_total = local_experts * groups
    capacity = 4 * token_count // expert_total
    slot_span = local_experts * capacity
    resid_wide = resid_in.astype(f32)
    inv_rms = lax.rsqrt(jnp.mean(resid_wide * resid_wide, axis=1, keepdims=True) + norm_eps)
    normed = (resid_wide * inv_rms * norm_gain).astype(bf16)
    mixed = gate_c.astype(f32) * values_u.astype(f32)
    earlier = passed_along(mixed[-2:], "sp", 1)
    experts = jnp.arange(expert_total, dtype=jnp.int32)[:, None]
    first, second = (routes[:, 0] == experts).astype(f32), (routes[:, 1] == experts).astype(f32)
    earlier_rows = jnp.arange(token_count)[:, None] < jnp.arange(token_count)[None, :]
    ahead = jnp.dot(
        (first + second).astype(bf16), earlier_rows.astype(bf16), preferred_element_type=f32
    )
    slot_of = [
        routes[:, k] * capacity + jnp.sum(hit * ahead, axis=0).astype(jnp.int32)
        for k, hit in enumerate((first, second))
    ]
    slots = jnp.arange(expert_total * capacity, dtype=jnp.int32)[:, None]
    named = [(slots == target[None, :]) for target in slot_of]
    pick = (named[0] | named[1]).astype(bf16)
    kind = lax.axis_index("tp") % 2
    scale = [jnp.where(kind == 1, route_weights[:, k], 1.0) for k in range(2)]
    weighted = jnp.where(named[0], scale[0], jnp.where(named[1], scale[1], 0.0)).astype(bf16)
    packed = jnp.dot(
        weighted, jnp.where(kind == 1, cotangent, normed), preferred_element_type=f32
    ).astype(bf16)
    both = dispatch(packed.reshape(groups, slot_span, model_width))
    entry_rows = both[0].reshape(groups * capacity, model_width)
    entry_cots = both[1].reshape(groups * capacity, model_width)
    grads_gate, grads_up, grads_down, terms = ([], [], [], [])
    grad_gate, grad_up, grad_down, partial_sum = expert_pass(
        entry_rows, entry_cots, gate_weight[0], up_weight[0], down_weight[0]
    )
    grads_gate.append(grad_gate)
    grads_up.append(grad_up)
    grads_down.append(grad_down)
    terms.append(partial_sum.astype(bf16).reshape(groups, capacity, model_width))
    expert_term = terms[0]
    summed = (
        lax.psum_scatter(expert_term, "tp", scatter_dimension=2, tiled=True)
        .astype(jnp.float32)
        .astype(bf16)
    )
    returned = lax.all_to_all(summed, "sp", split_axis=0, concat_axis=0, tiled=True).reshape(
        expert_total * capacity, model_width // lanes
    )
    slot_sum = jnp.einsum("jt,jd->td", pick, returned, preferred_element_type=f32)
    dnormed = lax.all_gather(
        slot_sum.astype(jnp.bfloat16), "tp", axis=1, tiled=True
    ).astype(jnp.float32)
    scaled = dnormed * norm_gain
    resid_grad = (
        cotangent.astype(f32)
        + inv_rms * scaled
        - resid_wide * inv_rms**3 * jnp.mean(scaled * resid_wide, axis=1, keepdims=True)
    )
    grad_resid = resid_grad.astype(bf16)
    extended = jnp.concatenate([earlier, mixed], axis=0)
    conv = (
        taps[0] * extended[:token_count]
        + taps[1] * extended[1 : token_count + 1]
        + taps[2] * extended[2 : token_count + 2]
    )
    merged = (gate_b.astype(f32) * conv).astype(bf16)
    grad_out_weight = sum_at_owner(
        jnp.einsum("td,tc->dc", grad_resid, merged, preferred_element_type=f32).astype(
            jnp.bfloat16
        ),
        "sp",
        0,
    )
    dmerged = jnp.dot(grad_resid, out_weight, preferred_element_type=f32)
    grad_gate_b = (dmerged * conv).astype(bf16)
    dconv = dmerged * gate_b.astype(f32)
    later = passed_along(dconv[:2], "sp", -1)
    extended_grad = jnp.concatenate([dconv, later], axis=0)
    dmixed = (
        taps[2] * extended_grad[:token_count]
        + taps[1] * extended_grad[1 : token_count + 1]
        + taps[0] * extended_grad[2 : token_count + 2]
    )
    grad_gate_c = (dmixed * values_u.astype(f32)).astype(bf16)
    grad_values = (dmixed * gate_c.astype(f32)).astype(bf16)
    return (
        jnp.stack(grads_gate),
        jnp.stack(grads_up),
        jnp.stack(grads_down),
        grad_resid,
        grad_out_weight,
        grad_gate_b,
        grad_gate_c,
        grad_values,
    )


def solution(mesh):
    placed = (
        P("sp", None),
        P("sp", None),
        P(),
        P("sp", None),
        P("sp", None),
        P("sp", None, "tp"),
        P("sp", None, "tp"),
        P("sp", "tp", None),
        P(None, "tp"),
        P("sp", "tp"),
        P("sp", "tp"),
        P("sp", "tp"),
        P(None, "tp"),
    )
    return jax.shard_map(
        on_device,
        mesh=mesh,
        in_specs=placed,
        out_specs=(
            P("sp", None, "tp"),
            P("sp", None, "tp"),
            P("sp", "tp", None),
            P("sp", None),
            P("sp", "tp"),
            P("sp", "tp"),
            P("sp", "tp"),
            P("sp", "tp"),
        ),
        check_vma=False,
    )
```

profile of v0, /device:TPU:1, one launch (start us, length us, event | category | flops | bytes accessed | tf_op | source)
XLA Modules:
  0.0 293.7 jit_solution(6065795146666523142)
XLA Ops:
  7.2 0.0 copy-start
  7.2 0.0 reduce-scatter.2.cloned.1.call-start
  7.2 1.9 fusion
  9.1 0.8 slice_reduce_fusion.1
  9.9 0.8 fusion.53
  10.7 0.2 select_reduce_fusion.1
  10.9 7.2 %convolution_convert_fusion = bf16[1536,2048]{1,0:T(8,128)(2,1)} fusion(bf16[384,2048]{1,0:T(8,128)(2,1)} %param.14, bf16[384,2048]{1,0:T(8,128)(2,1)} %param.13, f32[2048]{0:T(1024)} %param.15, f32[384]{0:T(512)S(1)} %get-tuple-element.27, pred[]{:T(512)S(6)} %eq.71, bf16[384]{0:T(512)(128)(2,1)S(1)} %get-tuple-element.11, s32[384]{0:T(512)S(1)} %get-tuple-element.28, ...), kind=kOutput, calls=%fused_computation.1 | convolution fusion | flops 2425356288 | bytes 9451521 | tf_op jit(solution)/shard_map/dot_general | solution.py:206
  18.1 95.8 %shard_map.188 = bf16[2,32,48,2048]{3,2,1,0:T(8,128)(2,1)} custom-call(bf16[32,48,2048]{2,1,0:T(8,128)(2,1)} %bitcast.53), custom_call_target="tpu_custom_call" | custom-call | tf_op jit(solution)/shard_map/pallas_call | solution.py:125
  113.8 5.9 %fusion.59 = (bf16[1,32,48,2048]{3,2,1,0:T(8,128)(2,1)S(1)}, bf16[1,32,48,2048]{3,2,1,0:T(8,128)(2,1)S(1)}) fusion(bf16[2,32,48,2048]{3,2,1,0:T(8,128)(2,1)} %shard_map.188), kind=kLoop, calls=%fused_computation.97 | loop fusion | bytes 25165824 | tf_op jit(solution)/shard_map/slice | solution.py:211
  119.7 0.0 copy-start.3
  119.7 0.0 copy-start.4
  119.7 0.0 copy-start.8
  119.7 1.9 fusion.28
  121.7 0.7 copy-done.3
  122.3 0.0 copy-done.8
  122.4 1.9 fusion.31
  124.2 0.0 copy-start.22
  124.2 0.2 copy-done.4
  124.4 0.5 copy-done.20
  124.9 2.5 multiply_convert_fusion.1
  127.4 0.0 copy-done.22
  127.5 1.8 fusion.26
  129.3 4.6 %add_convert_fusion = bf16[1536,2048]{1,0:T(8,128)(2,1)} fusion(f32[1536,2048]{1,0:T(8,128)S(1)} %fusion.26, bf16[1536,256]{1,0:T(8,128)(2,1)S(1)} %get-tuple-element.20, bf16[1,2048,256]{2,1,0:T(8,128)(2,1)S(1)} %copy-done.8), kind=kOutput, calls=%fused_computation | convolution fusion | flops 1616904192 | bytes 20709376 | tf_op jit(solution)/shard_map/rf,df->rd/dot_general | solution.py:155
  133.9 0.0 reduce-scatter.2.cloned.1.call-update
  133.9 0.0 all-gather.2.cloned.1.call-start
  133.9 66.2 %reduce-scatter.2.cloned.1.call-done = bf16[32,48,512]{2,1,0:T(8,128)(2,1)} async-done(((bf16[32,48,2048]{2,1,0:T(8,128)(2,1)}), bf16[32,48,512]{2,1,0:T(8,128)(2,1)}) %reduce-scatter.2.cloned.1.call-update) | async-done | bytes 1572880 | tf_op jit(solution)/shard_map/reduce_scatter | solution.py:222
  200.1 30.4 %all_to_all.10 = bf16[32,48,512]{2,1,0:T(8,128)(2,1)S(1)} all-to-all(bf16[32,48,512]{2,1,0:T(8,128)(2,1)} %reduce-scatter.2.cloned.1.call-done), channel_id=1, replica_groups=mesh['sp'=32,'tp'=4] {'sp'}, dimensions={0} | all-to-all | bytes 3145728 | tf_op jit(solution)/shard_map/all_to_all | solution.py:226
  230.6 1.6 fusion.16
  232.2 0.0 all-gather.2.cloned.1.call-update
  232.2 0.0 copy-done.9
  232.2 0.0 copy-done.11
  232.2 0.0 slice-start
  232.3 3.0 %collective-permute-start = (f32[2,256]{1,0:T(2,128)S(1)}, f32[2,256]{1,0:T(2,128)S(1)}, u32[]{:S(2)}, u32[]{:S(2)}) collective-permute-start(f32[2,256]{1,0:T(2,128)S(1)} %slice.65), channel_id=1, source_target_pairs={{0,4},{4,8},{8,12},{12,16},{16,20},{20,24},{24,28},{28,32},{32,36}... | collective-permute-start | bytes 6152 | tf_op jit(solution)/shard_map/ppermute | solution.py:14
  235.2 0.0 copy-done.16
  235.3 0.0 slice-start.1
  235.3 0.0 copy-start.21
  235.3 0.0 copy-start.23
  235.3 6.4 %convolution_bitcast_fusion.2 = f32[1,2048,256]{2,1,0:T(8,128)} fusion(bf16[1536,2048]{1,0:T(8,128)(2,1)} %bitcast.47, bf16[1536,256]{1,0:T(8,128)(2,1)S(1)} %get-tuple-element.21), kind=kOutput, calls=%fused_computation.16 | convolution fusion | flops 1610612736 | bytes 9175040 | tf_op jit(solution)/shard_map/rd,rf->df/dot_general | solution.py:153
  241.7 0.0 slice-done
  241.7 0.0 copy-start.2
  241.7 0.0 copy-start.15
  241.7 3.2 %convolution_bitcast_fusion = f32[1,256,2048]{2,1,0:T(8,128)} fusion(bf16[1536,2048]{1,0:T(8,128)(2,1)S(1)} %bitcast.52, f32[1536,256]{1,0:T(8,128)S(1)} %copy-done.23, f32[1536,256]{1,0:T(8,128)S(1)} %copy-done.21), kind=kOutput, calls=%fused_computation.14 | convolution fusion | flops 1612972032 | bytes 11534336 | tf_op jit(solution)/shard_map/rf,rd->fd/dot_general | solution.py:149
  244.9 9.6 %all-gather.2.cloned.1.call-done = bf16[384,2048]{1,0:T(8,128)(2,1)} async-done(((bf16[384,512]{1,0:T(8,128)(2,1)}), bf16[384,2048]{1,0:T(8,128)(2,1)}) %all-gather.2.cloned.1.call-update) | async-done | bytes 1572880 | tf_op jit(solution)/shard_map/all_gather | solution.py:230
  254.5 2.1 fusion.6
  256.7 0.2 copy-done.6
  256.9 1.0 fusion.5
  257.9 0.0 copy-start.7
  257.9 0.0 collective-permute-done
  257.9 0.2 copy-done.18
  258.1 0.0 copy-done.19
  258.1 1.3 multiply_convert_fusion.4
  259.4 1.8 convolution_convert_fusion.1
  261.1 7.9 %all-to-all-start.1 = ((bf16[32,64,256]{2,1,0:T(8,128)(2,1)}), bf16[32,64,256]{2,1,0:T(8,128)(2,1)S(1)}, u32[]{:S(2)}, u32[]{:S(2)}) async-start(bf16[32,64,256]{2,1,0:T(8,128)(2,1)} %bitcast.14), calls=%async_computation.2 | async-start | bytes 2097152 | tf_op jit(solution)/shard_map/all_to_all | solution.py:24
  269.0 0.0 copy-start.12
  269.0 0.0 copy-start.10
  269.1 2.3 collective-permute-start.1
  271.3 0.0 copy-start.1
  271.4 6.1 %convolution_bitcast_fusion.1 = f32[1,2048,256]{2,1,0:T(8,128)} fusion(bf16[1536,2048]{1,0:T(8,128)(2,1)} %bitcast.48, bf16[1536,256]{1,0:T(8,128)(2,1)S(1)} %get-tuple-element.20), kind=kOutput, calls=%fused_computation.15 | convolution fusion | flops 1610612736 | bytes 9175040 | tf_op jit(solution)/shard_map/rd,rf->df/dot_general | solution.py:154
  277.4 5.5 %collective-permute-done.1 = f32[2,256]{1,0:T(2,128)S(1)} collective-permute-done((f32[2,256]{1,0:T(2,128)S(1)}, f32[2,256]{1,0:T(2,128)S(1)}, u32[]{:S(2)}, u32[]{:S(2)}) %collective-permute-start.1) | collective-permute-done | bytes 2080 | tf_op jit(solution)/shard_map/ppermute | solution.py:14
  283.0 0.8 fusion.45
  283.8 0.0 copy-done.10
  283.8 0.7 fusion.46
  284.5 1.5 all-to-all-done.1
  286.0 0.8 convert_reduce_fusion
  (32 shorter events, 0.1 us)
Async XLA Ops:
  7.2 112.5 %copy-start = (bf16[1,2048,256]{2,1,0:T(8,128)(2,1)S(1)}, bf16[1,2048,256]{2,1,0:T(8,128)(2,1)}, u32[]{:S(2)}) copy-start(bf16[1,2048,256]{2,1,0:T(8,128)(2,1)} %param.18) | copy-start | bytes 3145732
  7.2 193.0 %reduce-scatter.2.cloned.1.call-start = ((), (), s32[]{:S(2)}) async-start(), calls=%async_computation.3 | async-start | bytes 7864320 | tf_op jit(solution)/shard_map/reduce_scatter | solution.py:222
  119.7 2.7 copy-start.3
  119.7 4.8 %copy-start.4 = (bf16[1,32,48,2048]{3,2,1,0:T(8,128)(2,1)}, bf16[1,32,48,2048]{3,2,1,0:T(8,128)(2,1)S(1)}, u32[]{:S(2)}) copy-start(bf16[1,32,48,2048]{3,2,1,0:T(8,128)(2,1)S(1)} %get-tuple-element.18) | copy-start | bytes 18874372
  119.7 2.6 copy-start.8
  122.3 2.6 copy-start.20
  122.4 2.6 copy-start.17
  124.2 3.2 %copy-start.22 = (f32[1536,256]{1,0:T(8,128)}, f32[1536,256]{1,0:T(8,128)S(1)}, u32[]{:S(2)}) copy-start(f32[1536,256]{1,0:T(8,128)S(1)} %fusion.31) | copy-start | bytes 4718596
  133.9 120.6 %all-gather.2.cloned.1.call-start = ((), (), s32[]{:S(2)}) async-start(), calls=%async_computation.4 | async-start | bytes 1966080 | tf_op jit(solution)/shard_map/all_gather | solution.py:230
  230.6 1.6 copy-start.9
  230.6 1.6 copy-start.11
  230.6 4.7 %copy-start.16 = (f32[3,256]{1,0:T(4,128)S(1)}, f32[3,256]{1,0:T(4,128)}, u32[]{:S(2)}) copy-start(f32[3,256]{1,0:T(4,128)} %param.25) | copy-start | bytes 9220
  232.2 9.5 %slice-start = ((s8[6291456]{0:T(1024)(128)(4,1)}), s8[4194304]{0:T(1024)(128)(4,1)S(1)}, s32[]{:S(2)}) async-start(s8[6291456]{0:T(1024)(128)(4,1)} %bitcast.50), calls=%async_computation.5 | async-start | bytes 8388608
  232.3 25.6 %collective-permute-start = (f32[2,256]{1,0:T(2,128)S(1)}, f32[2,256]{1,0:T(2,128)S(1)}, u32[]{:S(2)}, u32[]{:S(2)}) collective-permute-start(f32[2,256]{1,0:T(2,128)S(1)} %slice.65), channel_id=1, source_target_pairs={{0,4},{4,8},{8,12},{12,16},{16,20},{20,24},{24,28},{28,32},{32,36}... | collective-permute-start | bytes 6152 | tf_op jit(solution)/shard_map/ppermute | solution.py:14
  235.3 6.4 %slice-start.1 = ((s8[6291456]{0:T(1024)(128)(4,1)}), s8[2097152]{0:T(1024)(128)(4,1)S(1)}, s32[]{:S(2)}) async-start(s8[6291456]{0:T(1024)(128)(4,1)} %bitcast.50), calls=%async_computation.6 | async-start | bytes 4194304
  235.3 6.4 %copy-start.21 = (f32[1536,256]{1,0:T(8,128)S(1)}, f32[1536,256]{1,0:T(8,128)}, u32[]{:S(2)}) copy-start(f32[1536,256]{1,0:T(8,128)} %copy-done.20) | copy-start | bytes 4718596
  235.3 6.4 %copy-start.23 = (f32[1536,256]{1,0:T(8,128)S(1)}, f32[1536,256]{1,0:T(8,128)}, u32[]{:S(2)}) copy-start(f32[1536,256]{1,0:T(8,128)} %copy-done.22) | copy-start | bytes 4718596
  241.7 12.8 %copy-start.2 = (bf16[384,2048]{1,0:T(8,128)(2,1)S(1)}, bf16[384,2048]{1,0:T(8,128)(2,1)}, u32[]{:S(2)}) copy-start(bf16[384,2048]{1,0:T(8,128)(2,1)} %param.13) | copy-start | bytes 4718596
  241.7 12.8 %copy-start.15 = (f32[2048]{0:T(1024)S(1)}, f32[2048]{0:T(1024)}, u32[]{:S(2)}) copy-start(f32[2048]{0:T(1024)} %param.15) | copy-start | bytes 24580
  254.5 2.2 copy-start.5
  254.5 2.4 copy-start.6
  256.8 1.2 copy-start.18
  256.9 1.2 copy-start.19
  257.9 1.5 copy-start.7
  259.4 9.6 %copy-start.13 = (f32[384,256]{1,0:T(8,128)}, f32[384,256]{1,0:T(8,128)S(1)}, u32[]{:S(2)}) copy-start(f32[384,256]{1,0:T(8,128)S(1)} %get-tuple-element.22) | copy-start | bytes 1179652
  261.1 24.9 %all-to-all-start.1 = ((bf16[32,64,256]{2,1,0:T(8,128)(2,1)}), bf16[32,64,256]{2,1,0:T(8,128)(2,1)S(1)}, u32[]{:S(2)}, u32[]{:S(2)}) async-start(bf16[32,64,256]{2,1,0:T(8,128)(2,1)} %bitcast.14), calls=%async_computation.2 | async-start | bytes 2097152 | tf_op jit(solution)/shard_map/all_to_all | solution.py:24
  269.0 13.9 %copy-start.12 = (bf16[384,256]{1,0:T(8,128)(2,1)S(1)}, bf16[384,256]{1,0:T(8,128)(2,1)}, u32[]{:S(2)}) copy-start(bf16[384,256]{1,0:T(8,128)(2,1)} %param.23) | copy-start | bytes 589828
  269.0 13.9 %copy-start.14 = (f32[384,256]{1,0:T(8,128)S(1)}, f32[384,256]{1,0:T(8,128)}, u32[]{:S(2)}) copy-start(f32[384,256]{1,0:T(8,128)} %copy-done.13) | copy-start | bytes 1179652
  269.0 14.8 %copy-start.10 = (bf16[384,256]{1,0:T(8,128)(2,1)S(1)}, bf16[384,256]{1,0:T(8,128)(2,1)}, u32[]{:S(2)}) copy-start(bf16[384,256]{1,0:T(8,128)(2,1)} %param.24) | copy-start | bytes 589828
  269.1 13.9 %collective-permute-start.1 = (f32[2,256]{1,0:T(2,128)S(1)}, f32[2,256]{1,0:T(2,128)S(1)}, u32[]{:S(2)}, u32[]{:S(2)}) collective-permute-start(f32[2,256]{1,0:T(2,128)S(1)} %slice.68), channel_id=1, source_target_pairs={{4,0},{8,4},{12,8},{16,12},{20,16},{24,20},{28,24},{32,28},{36,32}... | collective-permute-start | bytes 6152 | tf_op jit(solution)/shard_map/ppermute | solution.py:14
  271.3 15.5 %copy-start.1 = (bf16[1,2048,256]{2,1,0:T(8,128)(2,1)S(1)}, bf16[1,2048,256]{2,1,0:T(8,128)(2,1)}, u32[]{:S(2)}) copy-start(bf16[1,2048,256]{2,1,0:T(8,128)(2,1)} %param.18) | copy-start | bytes 3145732
Sparse Core Ops, SparseCore 0:
  134.0 66.0 reduce-scatter.1
  232.3 22.1 all-gather.1
where the time goes:
time: 294 us
  Pallas kernels  95.8 us (33%)
  waiting for transfers between devices  82.8 us (28%)
  matrix products  40.3 us (14%)
  blocking collectives  30.4 us (10%)
  between operations  14.4 us (5%)
  starting transfers between devices  13.2 us (4%)
  local copies, waits for them, and re-layouts  8.5 us (3%)
  other arithmetic  8.24 us (3%)
    pallas_call x1, Pallas kernels, dispatch(): pl.pallas_call(dispatch_kernel, out_shape=jax.ShapeDtypeStruct((2,) + pac...  95.8 us
    reduce_scatter x1, waiting for transfers between devices, on_device(): lax.psum_scatter(expert_term, 'tp', scatter_dimension=2, tiled=True)  66.2 us
    all_to_all x1, blocking collectives, on_device(): lax.all_to_all(summed, 'sp', split_axis=0, concat_axis=0, tiled=True)  30.4 us
    all_gather x1, waiting for transfers between devices, on_device(): lax.all_gather(slot_sum.astype(jnp.bfloat16), 'tp', axis=1, tiled=True)  9.56 us
    all_to_all x1, starting transfers between devices, sum_at_owner(): tiles = lax.all_to_all(cut_along(array, dim, size), axis, 0, 0, tiled=True)  7.87 us
    dot_general x1, matrix products, on_device(): jnp.dot(weighted, jnp.where(kind == 1, cotangent, normed), preferred_elem...  7.17 us
    dot_general x1, matrix products, expert_pass(): jnp.einsum('rd,rf->df', entry_rows, dgate, preferred_element_type=f32)  6.35 us
    dot_general x1, matrix products, expert_pass(): jnp.einsum('rd,rf->df', entry_rows, dup, preferred_element_type=f32)  6.09 us
  transfers between devices with their start and end apart: 5, of which 4 were waited for; matrix products, arithmetic and copies ran while one was open for 7% of the time, Pallas kernels for 0%

commit v1 on v0

v1 whole, which is shorter than its diff:
```python
import jax
import jax.numpy as jnp
from jax import lax
from jax.experimental import pallas as pl
from jax.experimental.pallas import tpu as pltpu
from jax.sharding import PartitionSpec as P

norm_eps = 1e-06


def passed_along(array, axis, by):
    size = lax.axis_size(axis)
    pairs = [(i, i + by) for i in range(size) if 0 <= i + by < size]
    return lax.ppermute(array, axis, pairs)


def cut_along(array, dim, size):
    before, after = (array.shape[:dim], array.shape[dim + 1 :])
    return jnp.moveaxis(array.reshape(*before, size, -1, *after), dim, 0)


def sum_at_owner(array, axis, dim):
    size = lax.axis_size(axis)
    tiles = lax.all_to_all(cut_along(array, dim, size), axis, 0, 0, tiled=True)
    return jnp.sum(tiles.astype(jnp.float32), axis=0)


MESH = pl.DeviceIdType.MESH
BF16 = jnp.bfloat16
F32 = jnp.float32
SLOTS = 48
PER_GROUP = 4
GROUP_ROWS = PER_GROUP * SLOTS
GROUPS = 32 // PER_GROUP


def offsets(k):
    m = 7 * k
    return (m // 8) % 4, (m // 2) % 4, m % 2


def moved(s, k, sign):
    z, y, c = s // 8, (s // 2) % 4, s % 2
    dz, dy, dc = offsets(k)
    z = lax.rem(z + 4 + sign * dz, 4)
    y = lax.rem(y + 4 + sign * dy, 4)
    return (z * 4 + y) * 2 + lax.rem(c + dc, 2)


def turn_of(expert, s):
    dz = (expert // 8 - s // 8) % 4
    dy = ((expert // 2) % 4 - (s // 2) % 4) % 4
    dc = (expert - s) % 2
    return (23 * (dz * 8 + dy * 2 + dc)) % 32


def dot_nn(a, b):
    return jnp.dot(a, b, preferred_element_type=F32)


def dot_nt(a, b):
    return lax.dot_general(a, b, (((1,), (1,)), ((), ())), preferred_element_type=F32)


def dot_tn(a, b):
    return lax.dot_general(a, b, (((0,), (0,)), ((), ())), preferred_element_type=F32)


def block(k):
    return pl.ds(pl.multiple_of(k * SLOTS, SLOTS), SLOTS)


def group(g):
    return pl.ds(pl.multiple_of(g * GROUP_ROWS, GROUP_ROWS), GROUP_ROWS)


def wide(j, size):
    return pl.ds(pl.multiple_of(j * size, size), size)


def experts_kernel(
    packed, gate_w, up_w, down_w, pick,
    grad_gate, grad_up, grad_down, total,
    both, part, swapped, summed, back, hidden, dgate, dup, half_out, half_in, half_own,
    far_send, far_recv, near_send, near_recv, swap_send, swap_recv,
    back_send, back_recv, half_send, half_recv, all_send, all_recv, own_sem,
):
    s, x = lax.axis_index("sp"), lax.axis_index("tp")
    kind = lax.rem(x, 2)
    high = x // 2
    right, left, across = lax.rem(x + 1, 4), lax.rem(x + 3, 4), lax.rem(x + 2, 4)
    sides = (right, left)
    given = (1 + 2 * kind, 2 - 2 * kind)
    kept = (2 * kind, 3 - 2 * kind)
    barrier = pltpu.get_barrier_semaphore()

    def greet(k, carry):
        pl.semaphore_signal(
            barrier, inc=1, device_id={"sp": moved(s, k, 1), "tp": x}, device_id_type=MESH
        )
        return carry

    lax.fori_loop(1, 32, greet, 0)
    for lane in (right, left, across):
        pl.semaphore_signal(barrier, inc=1, device_id={"sp": s, "tp": lane}, device_id_type=MESH)
    pl.semaphore_wait(barrier, 34)

    def far(k):
        return pltpu.make_async_remote_copy(
            src_ref=packed.at[block(k)],
            dst_ref=both.at[kind, block(k)],
            send_sem=far_send.at[k],
            recv_sem=far_recv.at[k],
            device_id={"sp": moved(s, k, 1), "tp": x},
            device_id_type=MESH,
        )

    def near(h, k, own=False):
        cols = pl.ds(h * 1024, 1024)
        return pltpu.make_async_remote_copy(
            src_ref=packed.at[block(0), cols] if own else both.at[kind, block(k), cols],
            dst_ref=both.at[kind, block(k), cols],
            send_sem=near_send.at[h, k],
            recv_sem=near_recv.at[h, k],
            device_id={"sp": s, "tp": sides[h]},
            device_id_type=MESH,
        )

    def swap(h, k):
        return pltpu.make_async_remote_copy(
            src_ref=part.at[block(k), wide(given[h], 512)],
            dst_ref=swapped.at[1 - h, block(k)],
            send_sem=swap_send.at[h, k],
            recv_sem=swap_recv.at[h, k],
            device_id={"sp": s, "tp": sides[h]},
            device_id_type=MESH,
        )

    def home(k):
        return pltpu.make_async_remote_copy(
            src_ref=summed.at[block(k)],
            dst_ref=back.at[block(k)],
            send_sem=back_send.at[k],
            recv_sem=back_recv.at[k],
            device_id={"sp": moved(s, k, -1), "tp": x},
            device_id_type=MESH,
        )

    def each(first, last, action):
        def body(k, carry):
            action(k)
            return carry

        lax.fori_loop(first, last, body, 0)

    keep = pltpu.make_async_copy(packed.at[block(0)], both.at[kind, block(0)], own_sem)
    each(1, 32, lambda k: far(k).start())
    keep.start()
    for h in range(2):
        near(h, 0, True).start()
    grad_gate[...] = jnp.zeros_like(grad_gate)
    grad_up[...] = jnp.zeros_like(grad_up)
    grad_down[...] = jnp.zeros_like(grad_down)
    keep.wait()

    def pass_on(k):
        far(k).wait_recv()
        for h in range(2):
            near(h, k).start()

    def arrived(k):
        for h in range(2):
            near(h, k).wait_recv()

    def expert(g):
        rows = group(g)
        row, cot = both[0, rows, :], both[1, rows, :]
        gate = dot_nn(row, gate_w[...])
        up = dot_nn(row, up_w[...])
        dhidden = dot_nt(cot, down_w[...])
        logistic = jax.nn.sigmoid(gate)
        activated = gate * logistic
        hidden[...] = (activated * up).astype(BF16)
        dgate[...] = (dhidden * up * logistic * (1.0 + gate * (1.0 - logistic))).astype(BF16)
        dup[...] = (dhidden * activated).astype(BF16)

        def tile(j):
            cols = wide(j, 512)
            part[rows, cols] = (
                dot_nt(dgate[...], gate_w[cols, :]) + dot_nt(dup[...], up_w[cols, :])
            ).astype(BF16)

        each(0, 4, tile)

    def weights(g):
        rows = group(g)

        def tile(j):
            cols = wide(j, 512)
            row = both[0, rows, cols]
            grad_gate[cols, :] += dot_tn(row, dgate[...])
            grad_up[cols, :] += dot_tn(row, dup[...])
            grad_down[:, cols] += dot_tn(hidden[...], both[1, rows, cols])

        each(0, 4, tile)

    def swap_arrived(k):
        for h in range(2):
            swap(h, k).wait_recv()

    def pair_sum(g):
        rows = group(g)
        for h in range(2):
            summed[rows, pl.ds(h * 512, 512)] = (
                part[rows, wide(kept[h], 512)].astype(F32) + swapped[h, rows, :].astype(F32)
            ).astype(BF16)

    def step(g, carry):
        first = g * PER_GROUP

        @pl.when(g < GROUPS)
        def _():
            each(jnp.maximum(first, 1), first + PER_GROUP, pass_on)

        @pl.when((g >= 1) & (g <= GROUPS))
        def _():
            each(first - PER_GROUP, first, arrived)
            expert(g - 1)

        @pl.when((g >= 2) & (g <= GROUPS + 1))
        def _():
            each(first - 2 * PER_GROUP, first - PER_GROUP, swap_arrived)
            pair_sum(g - 2)

        @pl.when((g >= 1) & (g <= GROUPS))
        def _():
            def send(k):
                for h in range(2):
                    swap(h, k).start()

            each(first - PER_GROUP, first, send)
            weights(g - 1)

        @pl.when((g >= 2) & (g <= GROUPS + 1))
        def _():
            each(jnp.maximum(first - 2 * PER_GROUP, 1), first - PER_GROUP, lambda k: home(k).start())

        return carry

    lax.fori_loop(0, GROUPS + 2, step, 0)
    back[block(0), :] = summed[block(0), :]
    each(1, 32, lambda k: home(k).wait_recv())

    def gathered(half, j):
        return dot_nn(pick[...], back[:, wide(half * 2 + j, 256)])

    for j in range(2):
        half_out[:, pl.ds(j * 256, 256)] = gathered(1 - high, j).astype(BF16)
    cross = pltpu.make_async_remote_copy(
        src_ref=half_out,
        dst_ref=half_in,
        send_sem=half_send,
        recv_sem=half_recv,
        device_id={"sp": s, "tp": across},
        device_id_type=MESH,
    )
    cross.start()
    for j in range(2):
        half_own[:, pl.ds(j * 256, 256)] = gathered(high, j)
    cross.wait()

    def quarter_of(lane):
        odd, upper = lax.rem(lane, 2), lane // 2
        return (1 - upper) * 2 * odd + upper * (3 - 2 * odd)

    total[:, wide(quarter_of(x), 512)] = (half_own[...] + half_in[...].astype(F32)).astype(BF16)
    rows_half = total.shape[0] // 2

    def share(n, owner, h, lane):
        piece = total.at[pl.ds(h * rows_half, rows_half), wide(quarter_of(owner), 512)]
        return pltpu.make_async_remote_copy(
            src_ref=piece,
            dst_ref=piece,
            send_sem=all_send.at[n],
            recv_sem=all_recv.at[n],
            device_id={"sp": s, "tp": lane},
            device_id_type=MESH,
        )

    shares = [
        share(0, x, 0, right),
        share(1, x, 1, right),
        share(2, x, 0, left),
        share(3, x, 1, left),
        share(4, left, 0, right),
        share(5, right, 1, left),
    ]
    for n in (0, 3, 1, 2):
        shares[n].start()
    shares[0].wait_recv()
    shares[4].start()
    shares[3].wait_recv()
    shares[5].start()
    for n in (1, 2, 4, 5):
        shares[n].wait_recv()
    for copy in shares:
        copy.wait_send()

    def finish(k):
        far(k).wait_send()
        home(k).wait_send()
        for h in range(2):
            near(h, k).wait_send()

    each(1, 32, finish)
    for h in range(2):
        near(h, 0, True).wait_send()

    def finish_swap(k):
        for h in range(2):
            swap(h, k).wait_send()

    each(0, 32, finish_swap)


def experts(packed, gate_w, up_w, down_w, pick, token_count):
    vmem = pl.BlockSpec(memory_space=pltpu.VMEM)
    slots, width = packed.shape
    hidden = gate_w.shape[1]
    return pl.pallas_call(
        experts_kernel,
        out_shape=[
            jax.ShapeDtypeStruct((width, hidden), F32),
            jax.ShapeDtypeStruct((width, hidden), F32),
            jax.ShapeDtypeStruct((hidden, width), F32),
            jax.ShapeDtypeStruct((token_count, width), BF16),
        ],
        in_specs=[pl.BlockSpec(memory_space=pl.ANY)] + [vmem] * 4,
        out_specs=[vmem] * 4,
        scratch_shapes=[
            pltpu.VMEM((2, slots, width), BF16),
            pltpu.VMEM((slots, width), BF16),
            pltpu.VMEM((2, slots, 512), BF16),
            pltpu.VMEM((slots, 1024), BF16),
            pltpu.VMEM((slots, 1024), BF16),
            pltpu.VMEM((GROUP_ROWS, hidden), BF16),
            pltpu.VMEM((GROUP_ROWS, hidden), BF16),
            pltpu.VMEM((GROUP_ROWS, hidden), BF16),
            pltpu.VMEM((token_count, 512), BF16),
            pltpu.VMEM((token_count, 512), BF16),
            pltpu.VMEM((token_count, 512), F32),
            pltpu.SemaphoreType.DMA((32,)),
            pltpu.SemaphoreType.DMA((32,)),
            pltpu.SemaphoreType.DMA((2, 32)),
            pltpu.SemaphoreType.DMA((2, 32)),
            pltpu.SemaphoreType.DMA((2, 32)),
            pltpu.SemaphoreType.DMA((2, 32)),
            pltpu.SemaphoreType.DMA((32,)),
            pltpu.SemaphoreType.DMA((32,)),
            pltpu.SemaphoreType.DMA,
            pltpu.SemaphoreType.DMA,
            pltpu.SemaphoreType.DMA((6,)),
            pltpu.SemaphoreType.DMA((6,)),
            pltpu.SemaphoreType.DMA,
        ],
        compiler_params=pltpu.CompilerParams(
            collective_id=0, has_side_effects=True, vmem_limit_bytes=58 * 2**20
        ),
    )(packed, gate_w, up_w, down_w, pick)


def on_device(
    resid_in,
    cotangent,
    norm_gain,
    routes,
    route_weights,
    gate_weight,
    up_weight,
    down_weight,
    out_weight,
    gate_b,
    gate_c,
    values_u,
    taps,
):
    f32 = jnp.float32
    bf16 = jnp.bfloat16
    token_count = resid_in.shape[0]
    groups = lax.axis_size("sp")
    expert_total = groups
    resid_wide = resid_in.astype(f32)
    inv_rms = lax.rsqrt(jnp.mean(resid_wide * resid_wide, axis=1, keepdims=True) + norm_eps)
    normed = (resid_wide * inv_rms * norm_gain).astype(bf16)
    mixed = gate_c.astype(f32) * values_u.astype(f32)
    earlier = passed_along(mixed[-2:], "sp", 1)
    names = jnp.arange(expert_total, dtype=jnp.int32)[:, None]
    first, second = (routes[:, 0] == names).astype(f32), (routes[:, 1] == names).astype(f32)
    order = jnp.arange(token_count)
    ahead = jnp.dot(
        (first + second).astype(bf16),
        (order[:, None] < order[None, :]).astype(bf16),
        preferred_element_type=f32,
    )
    s, kind = lax.axis_index("sp"), lax.axis_index("tp") % 2
    slot_of = [
        turn_of(routes[:, k], s) * SLOTS + jnp.sum(hit * ahead, axis=0).astype(jnp.int32)
        for k, hit in enumerate((first, second))
    ]
    slots = jnp.arange(expert_total * SLOTS, dtype=jnp.int32)
    named = [slots[:, None] == target[None, :] for target in slot_of]
    scale = [jnp.where(kind == 1, route_weights[:, k], 1.0) for k in range(2)]
    weighted = jnp.where(named[0], scale[0], jnp.where(named[1], scale[1], 0.0)).astype(bf16)
    packed = jnp.dot(
        weighted, jnp.where(kind == 1, cotangent, normed), preferred_element_type=f32
    ).astype(bf16)
    pick = (
        (slots[None, :] == slot_of[0][:, None]) | (slots[None, :] == slot_of[1][:, None])
    ).astype(bf16)
    grad_gate, grad_up, grad_down, dnormed = experts(
        packed, gate_weight[0], up_weight[0], down_weight[0], pick, token_count
    )
    dnormed = dnormed.astype(f32)
    scaled = dnormed * norm_gain
    resid_grad = (
        cotangent.astype(f32)
        + inv_rms * scaled
        - resid_wide * inv_rms**3 * jnp.mean(scaled * resid_wide, axis=1, keepdims=True)
    )
    grad_resid = resid_grad.astype(bf16)
    extended = jnp.concatenate([earlier, mixed], axis=0)
    conv = (
        taps[0] * extended[:token_count]
        + taps[1] * extended[1 : token_count + 1]
        + taps[2] * extended[2 : token_count + 2]
    )
    merged = (gate_b.astype(f32) * conv).astype(bf16)
    grad_out_weight = sum_at_owner(
        jnp.einsum("td,tc->dc", grad_resid, merged, preferred_element_type=f32).astype(
            jnp.bfloat16
        ),
        "sp",
        0,
    )
    dmerged = jnp.dot(grad_resid, out_weight, preferred_element_type=f32)
    grad_gate_b = (dmerged * conv).astype(bf16)
    dconv = dmerged * gate_b.astype(f32)
    later = passed_along(dconv[:2], "sp", -1)
    extended_grad = jnp.concatenate([dconv, later], axis=0)
    dmixed = (
        taps[2] * extended_grad[:token_count]
        + taps[1] * extended_grad[1 : token_count + 1]
        + taps[0] * extended_grad[2 : token_count + 2]
    )
    grad_gate_c = (dmixed * values_u.astype(f32)).astype(bf16)
    grad_values = (dmixed * gate_c.astype(f32)).astype(bf16)
    return (
        grad_gate[None],
        grad_up[None],
        grad_down[None],
        grad_resid,
        grad_out_weight,
        grad_gate_b,
        grad_gate_c,
        grad_values,
    )


def solution(mesh):
    placed = (
        P("sp", None),
        P("sp", None),
        P(),
        P("sp", None),
        P("sp", None),
        P("sp", None, "tp"),
        P("sp", None, "tp"),
        P("sp", "tp", None),
        P(None, "tp"),
        P("sp", "tp"),
        P("sp", "tp"),
        P("sp", "tp"),
        P(None, "tp"),
    )
    return jax.shard_map(
        on_device,
        mesh=mesh,
        in_specs=placed,
        out_specs=(
            P("sp", None, "tp"),
            P("sp", None, "tp"),
            P("sp", "tp", None),
            P("sp", None),
            P("sp", "tp"),
            P("sp", "tp"),
            P("sp", "tp"),
            P("sp", "tp"),
        ),
        check_vma=False,
    )
```

time: 294 us -> 227 us (0.77)
  Pallas kernels: 95.8 us -> 169 us
  waiting for transfers between devices: 82.8 us -> 13.3 us
  matrix products: 40.3 us -> 8.99 us
  blocking collectives: 30.4 us -> 0 us
  between operations: 14.4 us -> 0.92 us
    pallas_call x1, Pallas kernels: 95.8 us -> 169 us  [experts(): pl.pallas_call(experts_kernel, out_shape=[jax.ShapeDtypeStruct((width, hi...]
    reduce_scatter x1 -> x0, waiting for transfers between devices: 66.2 us -> none  [on_device(): lax.psum_scatter(expert_term, 'tp', scatter_dimension=2, tiled=True)]
    all_to_all x1 -> x0, blocking collectives: 30.4 us -> none  [on_device(): lax.all_to_all(summed, 'sp', split_axis=0, concat_axis=0, tiled=True)]
    dot_general x10 -> x1, matrix products: 30.1 us -> 0.19 us  [on_device(): jnp.dot((first + second).astype(bf16), (order[:, None] < order[None, :])....]
    all_gather x1 -> x0, waiting for transfers between devices: 9.56 us -> none  [on_device(): lax.all_gather(slot_sum.astype(jnp.bfloat16), 'tp', axis=1, tiled=True)]
    ppermute x2, waiting for transfers between devices: 5.51 us -> 11.8 us  [passed_along(): return lax.ppermute(array, axis, pairs)]
    slice x2 -> x1, local copies, waits for them, and re-layouts: 6.63 us -> 0.78 us  [on_device(): routes[:, k]]
    unnamed x52 -> x31, local copies, waits for them, and re-layouts: 1.86 us -> 7.1 us
  transfers between devices with their start and end apart: 5 -> 3, of which waited for: 4 -> 2; matrix products, arithmetic and copies ran while one was open for 7% -> 7% of each run, Pallas kernels for 0% -> 75%
where the time goes in v1:
time: 227 us; the launch traced here: 226 us
  Pallas kernels  169 us (74%)
  starting transfers between devices  16 us (7%)
  waiting for transfers between devices  13.3 us (6%)
  other arithmetic  10.1 us (4%)
  matrix products  8.99 us (4%)
  local copies, waits for them, and re-layouts  7.89 us (3%)
    pallas_call x1, Pallas kernels, experts(): pl.pallas_call(experts_kernel, out_shape=[jax.ShapeDtypeStruct((width, hi...  169 us
    ppermute x2, waiting for transfers between devices, passed_along(): return lax.ppermute(array, axis, pairs)  11.8 us
    all_to_all x1, starting transfers between devices, sum_at_owner(): tiles = lax.all_to_all(cut_along(array, dim, size), axis, 0, 0, tiled=True)  9.24 us
    unnamed x31, local copies, waits for them, and re-layouts  7.1 us
    ppermute x2, starting transfers between devices, passed_along(): return lax.ppermute(array, axis, pairs)  6.73 us
    dot_general x1, matrix products, on_device(): jnp.dot(weighted, jnp.where(kind == 1, cotangent, normed), preferred_elem...  5.8 us
  transfers between devices with their start and end apart: 3, of which 2 were waited for; matrix products, arithmetic and copies ran while one was open for 7% of the time, Pallas kernels for 75%

profile of v1, /device:TPU:1, one launch (start us, length us, event | category | flops | bytes accessed | tf_op | source)
XLA Modules:
  0.0 226.2 jit_solution(9593648920849457383)
XLA Ops:
  0.6 0.0 copy-start
  0.6 0.0 copy-start.10
  0.7 0.0 copy-start.1
  0.7 0.0 copy-start.11
  0.7 0.0 copy-start.9
  0.7 1.2 convert_multiply_fusion.6
  1.9 4.6 %collective-permute-start = (f32[2,256]{1,0:T(2,128)S(1)}, f32[2,256]{1,0:T(2,128)S(1)}, u32[]{:S(2)}, u32[]{:S(2)}) collective-permute-start(f32[2,256]{1,0:T(2,128)S(1)} %slice.57), channel_id=1, source_target_pairs={{0,4},{4,8},{8,12},{12,16},{16,20},{20,24},{24,28},{28,32},{32,36}... | collective-permute-start | bytes 6152 | tf_op jit(solution)/shard_map/ppermute | solution.py:14
  6.6 0.8 slice_reduce_fusion.1
  7.3 1.8 fusion
  9.1 0.2 select_reduce_fusion.1
  9.4 0.0 copy-done.11
  9.5 0.0 copy-done.10
  9.5 0.1 fusion.95
  9.6 1.4 fusion.8.pick
  11.0 0.0 copy-done.1
  11.0 0.0 copy-done.9
  11.0 5.8 %convolution_convert_fusion.packed = bf16[1536,2048]{1,0:T(8,128)(2,1)} fusion(bf16[384,2048]{1,0:T(8,128)(2,1)} %param.14, bf16[384,2048]{1,0:T(8,128)(2,1)S(1)} %copy-done.1, f32[2048]{0:T(1024)S(1)} %copy-done.9, f32[384]{0:T(512)S(1)} %get-tuple-element.33, pred[]{:T(512)S(6)} %eq.114, bf16[384]{0:T(512)(128)(2,1)S(1)} %get-tuple-element.21, ...), kind=kOutput, calls=%fused_computation | convolution fusion | flops 2425356288 | bytes 9451521 | tf_op jit(solution)/shard_map/dot_general | solution.py:414
  16.8 169.0 %shard_map.188 = (f32[2048,256]{1,0:T(8,128)}, f32[2048,256]{1,0:T(8,128)}, f32[256,2048]{1,0:T(8,128)}, bf16[384,2048]{1,0:T(8,128)(2,1)}) custom-call(bf16[1536,2048]{1,0:T(8,128)(2,1)} %convolution_convert_fusion.packed, bf16[2048,256]{1,0:T(8,128)(2,1)} %bitcast.17, bf16[2048,256]{1,0:T(8,128)(2,1)} %bitcast.18, bf16[256,2048]{1,0:T(8,128)(2,1)} %bitcast.19, ...), custom_call_target="tpu_custom_call" | custom-call | tf_op jit(solution)/shard_map/pallas_call | solution.py:330
  185.8 0.0 copy-start.2
  185.8 0.0 copy-start.5
  185.8 2.1 fusion.6
  187.9 0.0 copy-done.2
  188.0 0.2 copy-done.5
  188.1 0.0 copy-start.12
  188.1 0.0 copy-start.13
  188.1 1.0 fusion.5
  189.2 0.0 copy-done.12
  189.2 0.0 copy-start.6
  189.2 0.0 collective-permute-done
  189.2 0.0 copy-done
  189.2 0.0 copy-done.13
  189.2 1.3 multiply_convert_fusion
  190.5 0.0 copy-done.6
  190.5 0.0 copy-start.8
  190.5 1.7 convolution_convert_fusion.1
  192.2 0.0 copy-start.7
  192.3 9.2 %all-to-all-start = ((bf16[32,64,256]{2,1,0:T(8,128)(2,1)}), bf16[32,64,256]{2,1,0:T(8,128)(2,1)S(1)}, u32[]{:S(2)}, u32[]{:S(2)}) async-start(bf16[32,64,256]{2,1,0:T(8,128)(2,1)} %bitcast.16), calls=%async_computation | async-start | bytes 2097152 | tf_op jit(solution)/shard_map/all_to_all | solution.py:24
  201.5 2.1 collective-permute-start.1
  203.7 11.8 %collective-permute-done.1 = f32[2,256]{1,0:T(2,128)S(1)} collective-permute-done((f32[2,256]{1,0:T(2,128)S(1)}, f32[2,256]{1,0:T(2,128)S(1)}, u32[]{:S(2)}, u32[]{:S(2)}) %collective-permute-start.1) | collective-permute-done | bytes 2080 | tf_op jit(solution)/shard_map/ppermute | solution.py:14
  215.4 0.0 copy-done.8
  215.5 0.8 fusion.29
  216.3 0.0 copy-done.7
  216.3 0.7 fusion.30
  217.0 1.5 all-to-all-done
  218.6 0.8 convert_reduce_fusion
  219.3 0.0 copy-start.4
  219.3 3.2 %copy.24 = f32[1,2048,256]{2,1,0:T(8,128)} copy(f32[1,2048,256]{2,1,0:T(8,128)} %bitcast.15) | data formatting | bytes 4194304
  222.5 0.0 copy-done.4
  222.5 0.0 copy-start.3
  222.5 1.3 copy.25
  223.8 1.0 copy-done.3
  224.9 1.3 copy.26
  (9 shorter events, 0.1 us)
Async XLA Ops:
  0.6 188.6 %copy-start = (bf16[2048,256]{1,0:T(8,128)(2,1)S(1)}, bf16[2048,256]{1,0:T(8,128)(2,1)}, u32[]{:S(2)}) copy-start(bf16[2048,256]{1,0:T(8,128)(2,1)} %param.21) | copy-start | bytes 3145732
  0.6 8.8 %copy-start.10 = (s32[384,2]{0,1:T(2,128)S(1)}, s32[384,2]{0,1:T(2,128)}, u32[]{:S(2)}) copy-start(s32[384,2]{0,1:T(2,128)} %param.16) | copy-start | bytes 9220
  0.7 10.3 %copy-start.1 = (bf16[384,2048]{1,0:T(8,128)(2,1)S(1)}, bf16[384,2048]{1,0:T(8,128)(2,1)}, u32[]{:S(2)}) copy-start(bf16[384,2048]{1,0:T(8,128)(2,1)} %param.13) | copy-start | bytes 4718596
  0.7 8.8 %copy-start.11 = (f32[384,2]{0,1:T(2,128)S(1)}, f32[384,2]{0,1:T(2,128)}, u32[]{:S(2)}) copy-start(f32[384,2]{0,1:T(2,128)} %param.17) | copy-start | bytes 9220
  0.7 10.3 %copy-start.9 = (f32[2048]{0:T(1024)S(1)}, f32[2048]{0:T(1024)}, u32[]{:S(2)}) copy-start(f32[2048]{0:T(1024)} %param.15) | copy-start | bytes 24580
  1.9 187.3 %collective-permute-start = (f32[2,256]{1,0:T(2,128)S(1)}, f32[2,256]{1,0:T(2,128)S(1)}, u32[]{:S(2)}, u32[]{:S(2)}) collective-permute-start(f32[2,256]{1,0:T(2,128)S(1)} %slice.57), channel_id=1, source_target_pairs={{0,4},{4,8},{8,12},{12,16},{16,20},{20,24},{24,28},{28,32},{32,36}... | collective-permute-start | bytes 6152 | tf_op jit(solution)/shard_map/ppermute | solution.py:14
  185.8 2.2 copy-start.2
  185.8 2.3 %copy-start.5 = (bf16[384,2048]{1,0:T(8,128)(2,1)S(1)}, bf16[384,2048]{1,0:T(8,128)(2,1)}, u32[]{:S(2)}) copy-start(bf16[384,2048]{1,0:T(8,128)(2,1)} %param.14) | copy-start | bytes 4718596
  188.1 1.0 copy-start.12
  188.1 1.1 copy-start.13
  189.2 1.3 copy-start.6
  190.5 24.9 %copy-start.8 = (bf16[384,256]{1,0:T(8,128)(2,1)S(1)}, bf16[384,256]{1,0:T(8,128)(2,1)}, u32[]{:S(2)}) copy-start(bf16[384,256]{1,0:T(8,128)(2,1)} %param.23) | copy-start | bytes 589828
  192.2 24.0 %copy-start.7 = (bf16[384,256]{1,0:T(8,128)(2,1)S(1)}, bf16[384,256]{1,0:T(8,128)(2,1)}, u32[]{:S(2)}) copy-start(bf16[384,256]{1,0:T(8,128)(2,1)} %param.24) | copy-start | bytes 589828
  192.3 26.3 %all-to-all-start = ((bf16[32,64,256]{2,1,0:T(8,128)(2,1)}), bf16[32,64,256]{2,1,0:T(8,128)(2,1)S(1)}, u32[]{:S(2)}, u32[]{:S(2)}) async-start(bf16[32,64,256]{2,1,0:T(8,128)(2,1)} %bitcast.16), calls=%async_computation | async-start | bytes 2097152 | tf_op jit(solution)/shard_map/all_to_all | solution.py:24
  201.5 13.9 %collective-permute-start.1 = (f32[2,256]{1,0:T(2,128)S(1)}, f32[2,256]{1,0:T(2,128)S(1)}, u32[]{:S(2)}, u32[]{:S(2)}) collective-permute-start(f32[2,256]{1,0:T(2,128)S(1)} %slice.60), channel_id=1, source_target_pairs={{4,0},{8,4},{12,8},{16,12},{20,16},{24,20},{28,24},{32,28},{36,32}... | collective-permute-start | bytes 6152 | tf_op jit(solution)/shard_map/ppermute | solution.py:14
  219.3 3.2 %copy-start.4 = (f32[2048,256]{1,0:T(8,128)S(1)}, f32[2048,256]{1,0:T(8,128)}, u32[]{:S(2)}) copy-start(f32[2048,256]{1,0:T(8,128)} %get-tuple-element.13) | copy-start | bytes 6291460
  222.5 2.3 %copy-start.3 = (f32[256,2048]{1,0:T(8,128)S(1)}, f32[256,2048]{1,0:T(8,128)}, u32[]{:S(2)}) copy-start(f32[256,2048]{1,0:T(8,128)} %get-tuple-element.14) | copy-start | bytes 6291460

commit v2 on v1

v2 whole, which is shorter than its diff:
```python
import jax
import jax.numpy as jnp
from jax import lax
from jax.experimental import pallas as pl
from jax.experimental.pallas import tpu as pltpu
from jax.sharding import PartitionSpec as P

norm_eps = 1e-06


MESH = pl.DeviceIdType.MESH
BF16 = jnp.bfloat16
F32 = jnp.float32
SLOTS = 48
PER_GROUP = 2
GROUP_ROWS = PER_GROUP * SLOTS
GROUPS = 32 // PER_GROUP


def offsets(k):
    m = 7 * k
    return (m // 8) % 4, (m // 2) % 4, m % 2


def moved(s, k, sign):
    z, y, c = s // 8, (s // 2) % 4, s % 2
    dz, dy, dc = offsets(k)
    z = lax.rem(z + 4 + sign * dz, 4)
    y = lax.rem(y + 4 + sign * dy, 4)
    return (z * 4 + y) * 2 + lax.rem(c + dc, 2)


def turn_of(expert, s):
    dz = (expert // 8 - s // 8) % 4
    dy = ((expert // 2) % 4 - (s // 2) % 4) % 4
    dc = (expert - s) % 2
    return (23 * (dz * 8 + dy * 2 + dc)) % 32


def dot_nn(a, b):
    return jnp.dot(a, b, preferred_element_type=F32)


def dot_nt(a, b):
    return lax.dot_general(a, b, (((1,), (1,)), ((), ())), preferred_element_type=F32)


def dot_tn(a, b):
    return lax.dot_general(a, b, (((0,), (0,)), ((), ())), preferred_element_type=F32)


def block(k):
    return pl.ds(pl.multiple_of(k * SLOTS, SLOTS), SLOTS)


def group(g):
    return pl.ds(pl.multiple_of(g * GROUP_ROWS, GROUP_ROWS), GROUP_ROWS)


def wide(j, size):
    return pl.ds(pl.multiple_of(j * size, size), size)


PARTNER = 23
EARLY = 5
EDGE = 8


def experts_kernel(
    resid, cots, gain, slot, weight, slot_col, gate_w, up_w, down_w, out_w,
    gate_b, gate_c, values, taps,
    grad_gate, grad_up, grad_down, grad_resid, grad_out, grad_b, grad_c, grad_values,
    both, part, extra, swapped, back, hidden, dgate, dup, half_out, half_in, half_own,
    normed, inverse, pick, total, mixed, conv, merged, dconv, staged, gathered,
    far_send, far_recv, near_send, near_recv, swap_send, swap_recv, back_send, back_recv,
    out_send, out_recv, all_send, all_recv,
    extra_send, extra_recv, half_send, half_recv, later_send, later_recv, sooner_send, sooner_recv,
):
    s, x = lax.axis_index("sp"), lax.axis_index("tp")
    kind = lax.rem(x, 2)
    high = x // 2
    right, left, across = lax.rem(x + 1, 4), lax.rem(x + 3, 4), lax.rem(x + 2, 4)
    sides = (right, left)
    given = (1 + 2 * kind, 2 - 2 * kind)
    kept = (2 * kind, 3 - 2 * kind)
    tokens = cots.shape[0]
    barrier = pltpu.get_barrier_semaphore()

    def each(first, last, action):
        def body(k, carry):
            action(k)
            return carry

        lax.fori_loop(first, last, body, 0)

    def greet(k):
        pl.semaphore_signal(
            barrier, inc=1, device_id={"sp": moved(s, k, 1), "tp": x}, device_id_type=MESH
        )

    each(1, 32, greet)
    for lane in (right, left, across):
        pl.semaphore_signal(barrier, inc=1, device_id={"sp": s, "tp": lane}, device_id_type=MESH)

    def remote(source, target, sent, received, sp, tp):
        return pltpu.make_async_remote_copy(
            src_ref=source,
            dst_ref=target,
            send_sem=sent,
            recv_sem=received,
            device_id={"sp": sp, "tp": tp},
            device_id_type=MESH,
        )

    def far(k):
        return remote(
            part.at[block(k)], both.at[kind, block(k)], far_send.at[k], far_recv.at[k],
            moved(s, k, 1), x,
        )

    def near(h, k):
        piece = both.at[kind, block(k), pl.ds(h * 1024, 1024)]
        return remote(piece, piece, near_send.at[h, k], near_recv.at[h, k], s, sides[h])

    def swap(h, k):
        return remote(
            part.at[block(k), wide(given[h], 512)],
            swapped.at[block(k), pl.ds((1 - h) * 512, 512)],
            swap_send.at[h, k], swap_recv.at[h, k], s, sides[h],
        )

    def home(k):
        return remote(
            swapped.at[block(k)], back.at[block(k)], back_send.at[k], back_recv.at[k],
            moved(s, k, -1), x,
        )

    other = remote(
        extra, both.at[1 - kind, block(PARTNER)], extra_send, extra_recv, moved(s, PARTNER, 1), x
    )
    later = remote(
        mixed.at[pl.ds(tokens, EDGE)], mixed.at[pl.ds(0, EDGE)], later_send, later_recv,
        jnp.minimum(s + 1, 31), x,
    )
    sooner = remote(
        dconv.at[pl.ds(0, EDGE)], dconv.at[pl.ds(tokens, EDGE)], sooner_send, sooner_recv,
        jnp.maximum(s - 1, 0), x,
    )

    def normalize(i):
        rows = wide(i, 64)
        held = resid[rows, :].astype(F32)
        scale = lax.rsqrt(jnp.mean(held * held, axis=1, keepdims=True) + norm_eps)
        normed[rows, :] = (held * scale * gain[...]).astype(BF16)
        inverse[rows, :] = jnp.broadcast_to(scale, (64, 128))

    each(0, tokens // 64, normalize)

    def pack(target, rows, first, count, is_cot):
        ids = lax.broadcasted_iota(jnp.int32, (count * SLOTS, tokens), 0) + first * SLOTS
        zero = jnp.zeros((count * SLOTS, tokens), F32)
        ones = jnp.ones((1, tokens), F32)
        value = [weight[k : k + 1, :] if is_cot else ones for k in range(2)]
        chosen = jnp.where(
            ids == slot[0:1, :], value[0], jnp.where(ids == slot[1:2, :], value[1], zero)
        ).astype(BF16)
        data = cots if is_cot else normed
        for j in range(4):
            cols = pl.ds(j * 512, 512)
            target[rows, cols] = dot_nn(chosen, data[:, cols]).astype(BF16)

    def pack_group(g):
        for option in range(2):

            @pl.when(kind == option)
            def _():
                rows = wide(g, 4 * SLOTS)
                pack(part, rows, g * 4, 4, option == 1)

    pack_group(0)
    mixed[pl.ds(EDGE, tokens), :] = gate_c[...].astype(F32) * values[...].astype(F32)
    pl.semaphore_wait(barrier, 34)

    def pass_on(k):
        far(k).wait_recv()

        @pl.when(k != PARTNER)
        def _():
            for h in range(2):
                near(h, k).start()

    def pack_and_send(g, carry):
        pack_group(g)
        each(jnp.maximum(g * 4 - 4, 1), g * 4, lambda k: far(k).start())

        @pl.when(g >= 4)
        def _():
            pass_on(g - 3)

        return carry

    lax.fori_loop(1, 8, pack_and_send, 0)
    each(28, 32, lambda k: far(k).start())

    @pl.when(s < 31)
    def _():
        later.start()

    for option in range(2):
        pack(both.at[option], pl.ds(0, SLOTS), 0, 1, option == 1)

        @pl.when(kind == option)
        def _():
            pack(extra, pl.ds(0, SLOTS), PARTNER, 1, option == 0)

    def arrived(k):
        @pl.when((k != PARTNER) & (k != 0))
        def _():
            for h in range(2):
                near(h, k).wait_recv()

        @pl.when(k == PARTNER)
        def _():
            other.wait_recv()

    def expert(g):
        rows = group(g)
        local = wide(lax.rem(g, 2), GROUP_ROWS)
        row, cot = both[0, rows, :], both[1, rows, :]
        gate = dot_nn(row, gate_w[...])
        up = dot_nn(row, up_w[...])
        dhidden = dot_nt(cot, down_w[...])
        logistic = jax.nn.sigmoid(gate)
        activated = gate * logistic
        hidden[local, :] = (activated * up).astype(BF16)
        dgate[local, :] = (dhidden * up * logistic * (1.0 + gate * (1.0 - logistic))).astype(BF16)
        dup[local, :] = (dhidden * activated).astype(BF16)

        def tile(j):
            cols = wide(j, 512)
            part[rows, cols] = (
                dot_nt(dgate[local, :], gate_w[cols, :]) + dot_nt(dup[local, :], up_w[cols, :])
            ).astype(BF16)

        each(0, 4, tile)

    def weights(chunk):
        rows = wide(chunk, 2 * GROUP_ROWS)

        def tile(j):
            cols = wide(j, 512)
            row = both[0, rows, cols]
            grad_gate[cols, :] += dot_tn(row, dgate[...])
            grad_up[cols, :] += dot_tn(row, dup[...])
            grad_down[:, cols] += dot_tn(hidden[...], both[1, rows, cols])

        each(0, 4, tile)

    def swap_arrived(k):
        for h in range(2):
            swap(h, k).wait_recv()

    def pair_sum(g):
        rows = group(g)
        for h in range(2):
            cols = pl.ds(h * 512, 512)
            swapped[rows, cols] = (
                part[rows, wide(kept[h], 512)].astype(F32) + swapped[rows, cols].astype(F32)
            ).astype(BF16)

    def make_pick():
        ids = lax.broadcasted_iota(jnp.int32, pick.shape, 1)
        hit = (ids == slot_col[:, 0:1]) | (ids == slot_col[:, 1:2])
        pick[...] = jnp.where(hit, 1.0, 0.0).astype(BF16)

    def make_conv():
        @pl.when(s == 0)
        def _():
            mixed[pl.ds(0, EDGE), :] = jnp.zeros((EDGE, mixed.shape[1]), F32)

        @pl.when(s > 0)
        def _():
            later.wait_recv()

        conv[...] = (
            taps[0:1, :] * mixed[pl.ds(EDGE - 2, tokens), :]
            + taps[1:2, :] * mixed[pl.ds(EDGE - 1, tokens), :]
            + taps[2:3, :] * mixed[pl.ds(EDGE, tokens), :]
        )
        merged[...] = (gate_b[...].astype(F32) * conv[...]).astype(BF16)

    def step(g, carry):
        first = g * PER_GROUP

        @pl.when(g < GROUPS)
        def _():
            each(jnp.maximum(first, EARLY), first + PER_GROUP, pass_on)

        @pl.when(g == 0)
        def _():
            other.start()
            grad_gate[...] = jnp.zeros_like(grad_gate)
            grad_up[...] = jnp.zeros_like(grad_up)
            grad_down[...] = jnp.zeros_like(grad_down)

        @pl.when((g >= 1) & (g <= GROUPS))
        def _():
            each(first - PER_GROUP, first, arrived)
            each(jnp.maximum(first - PER_GROUP, 1), first, lambda k: far(k).wait_send())
            expert(g - 1)

        @pl.when((g >= 2) & (g <= GROUPS + 1))
        def _():
            each(first - 2 * PER_GROUP, first - PER_GROUP, swap_arrived)
            pair_sum(g - 2)

        @pl.when((g >= 1) & (g <= GROUPS))
        def _():
            def send(k):
                for h in range(2):
                    swap(h, k).start()

            each(first - PER_GROUP, first, send)

        @pl.when((g >= 2) & (g < GROUPS) & (lax.rem(g, 2) == 0))
        def _():
            weights(g // 2 - 1)

        @pl.when(g == 3)
        def _():
            make_pick()

        @pl.when(g == 5)
        def _():
            make_conv()

        @pl.when((g >= 2) & (g <= GROUPS + 1))
        def _():
            each(jnp.maximum(first - 2 * PER_GROUP, 1), first - PER_GROUP, lambda k: home(k).start())

        return carry

    lax.fori_loop(0, GROUPS + 2, step, 0)
    back[block(0), :] = swapped[block(0), :]
    weights(GROUPS // 2 - 1)
    each(1, 32, lambda k: home(k).wait_recv())

    def summed(half, j):
        return dot_nn(pick[...], back[:, wide(half * 2 + j, 256)])

    for j in range(2):
        half_out[:, pl.ds(j * 256, 256)] = summed(1 - high, j).astype(BF16)
    cross = remote(half_out, half_in, half_send, half_recv, s, across)
    cross.start()
    for j in range(2):
        half_own[:, pl.ds(j * 256, 256)] = summed(high, j)
    cross.wait()

    def quarter_of(lane):
        odd, upper = lax.rem(lane, 2), lane // 2
        return (1 - upper) * 2 * odd + upper * (3 - 2 * odd)

    total[:, wide(quarter_of(x), 512)] = (half_own[...] + half_in[...].astype(F32)).astype(BF16)

    def share(n, owner, h, lane):
        piece = total.at[pl.ds(h * (tokens // 2), tokens // 2), wide(quarter_of(owner), 512)]
        return remote(piece, piece, all_send.at[n], all_recv.at[n], s, lane)

    shares = [
        share(0, x, 0, right),
        share(1, x, 1, right),
        share(2, x, 0, left),
        share(3, x, 1, left),
        share(4, left, 0, right),
        share(5, right, 1, left),
    ]
    for n in (0, 3, 1, 2):
        shares[n].start()
    shares[0].wait_recv()
    shares[4].start()
    shares[3].wait_recv()
    shares[5].start()
    for n in (1, 2, 4, 5):
        shares[n].wait_recv()
    for copy in shares:
        copy.wait_send()

    def resid_tile(i):
        rows = wide(i, 64)
        scaled = total[rows, :].astype(F32) * gain[...]
        held = resid[rows, :].astype(F32)
        scale = inverse[rows, 0:1]
        mean = jnp.mean(scaled * held, axis=1, keepdims=True)
        grad_resid[rows, :] = (
            cots[rows, :].astype(F32) + scale * scaled - held * (scale * scale * scale * mean)
        ).astype(BF16)

    each(0, tokens // 64, resid_tile)
    for j in range(4):
        cols = pl.ds(j * 512, 512)
        staged[cols, :] = dot_tn(grad_resid[:, cols], merged[...]).astype(BF16)
    share_rows = grad_out.shape[0]

    def give(k):
        owner = moved(s, k, 1)
        return remote(
            staged.at[wide(owner, share_rows)], gathered.at[k], out_send.at[k], out_recv.at[k],
            owner, x,
        )

    dmerged = dot_nn(grad_resid[...], out_w[...])
    dconv[pl.ds(0, tokens), :] = dmerged * gate_b[...].astype(F32)
    grad_b[...] = (dmerged * conv[...]).astype(BF16)
    each(1, 32, lambda k: give(k).start())

    @pl.when(s > 0)
    def _():
        sooner.start()

    @pl.when(s == 31)
    def _():
        dconv[pl.ds(tokens, EDGE), :] = jnp.zeros((EDGE, dconv.shape[1]), F32)

    gathered[0] = staged[wide(s, share_rows), :]

    def finish(k):
        home(k).wait_send()

        @pl.when(k != PARTNER)
        def _():
            for h in range(2):
                near(h, k).wait_send()

    each(1, 32, finish)

    def finish_swap(k):
        for h in range(2):
            swap(h, k).wait_send()

    each(0, 32, finish_swap)
    other.wait_send()

    @pl.when(s < 31)
    def _():
        later.wait_send()
        sooner.wait_recv()

    dmixed = (
        taps[2:3, :] * dconv[pl.ds(0, tokens), :]
        + taps[1:2, :] * dconv[pl.ds(1, tokens), :]
        + taps[0:1, :] * dconv[pl.ds(2, tokens), :]
    )
    grad_c[...] = (dmixed * values[...].astype(F32)).astype(BF16)
    grad_values[...] = (dmixed * gate_c[...].astype(F32)).astype(BF16)
    each(1, 32, lambda k: give(k).wait_recv())
    grad_out[...] = jnp.sum(gathered[...].astype(F32), axis=0)
    each(1, 32, lambda k: give(k).wait_send())

    @pl.when(s > 0)
    def _():
        sooner.wait_send()


def on_device(
    resid_in,
    cotangent,
    norm_gain,
    routes,
    route_weights,
    gate_weight,
    up_weight,
    down_weight,
    out_weight,
    gate_b,
    gate_c,
    values_u,
    taps,
):
    tokens, width = resid_in.shape
    hidden, channels = gate_weight.shape[2], gate_b.shape[1]
    experts = lax.axis_size("sp")
    slots = experts * SLOTS
    names = jnp.arange(experts, dtype=jnp.int32)[:, None]
    first, second = (routes[:, 0] == names).astype(F32), (routes[:, 1] == names).astype(F32)
    order = jnp.arange(tokens)
    ahead = jnp.dot(
        (first + second).astype(BF16),
        (order[:, None] < order[None, :]).astype(BF16),
        preferred_element_type=F32,
    )
    s = lax.axis_index("sp")
    slot = jnp.stack(
        [
            turn_of(routes[:, k], s) * SLOTS + jnp.sum(hit * ahead, axis=0).astype(jnp.int32)
            for k, hit in enumerate((first, second))
        ]
    )
    vmem = pl.BlockSpec(memory_space=pltpu.VMEM)
    dma = pltpu.SemaphoreType.DMA
    outs = pl.pallas_call(
        experts_kernel,
        out_shape=[
            jax.ShapeDtypeStruct((width, hidden), F32),
            jax.ShapeDtypeStruct((width, hidden), F32),
            jax.ShapeDtypeStruct((hidden, width), F32),
            jax.ShapeDtypeStruct((tokens, width), BF16),
            jax.ShapeDtypeStruct((width // experts, channels), F32),
            jax.ShapeDtypeStruct((tokens, channels), BF16),
            jax.ShapeDtypeStruct((tokens, channels), BF16),
            jax.ShapeDtypeStruct((tokens, channels), BF16),
        ],
        in_specs=[vmem] * 14,
        out_specs=[vmem] * 8,
        scratch_shapes=[
            pltpu.VMEM((2, slots, width), BF16),
            pltpu.VMEM((slots, width), BF16),
            pltpu.VMEM((SLOTS, width), BF16),
            pltpu.VMEM((slots, 1024), BF16),
            pltpu.VMEM((slots, 1024), BF16),
            pltpu.VMEM((2 * GROUP_ROWS, hidden), BF16),
            pltpu.VMEM((2 * GROUP_ROWS, hidden), BF16),
            pltpu.VMEM((2 * GROUP_ROWS, hidden), BF16),
            pltpu.VMEM((tokens, 512), BF16),
            pltpu.VMEM((tokens, 512), BF16),
            pltpu.VMEM((tokens, 512), F32),
            pltpu.VMEM((tokens, width), BF16),
            pltpu.VMEM((tokens, 128), F32),
            pltpu.VMEM((tokens, slots), BF16),
            pltpu.VMEM((tokens, width), BF16),
            pltpu.VMEM((tokens + EDGE, channels), F32),
            pltpu.VMEM((tokens, channels), F32),
            pltpu.VMEM((tokens, channels), BF16),
            pltpu.VMEM((tokens + EDGE, channels), F32),
            pltpu.VMEM((width, channels), BF16),
            pltpu.VMEM((experts, width // experts, channels), BF16),
        ]
        + [dma((32,)), dma((32,)), dma((2, 32)), dma((2, 32)), dma((2, 32)), dma((2, 32))]
        + [dma((32,))] * 4
        + [dma((6,))] * 2
        + [dma] * 8,
        compiler_params=pltpu.CompilerParams(
            collective_id=0, has_side_effects=True, vmem_limit_bytes=63 * 2**20
        ),
    )(
        resid_in, cotangent, norm_gain[None], slot, route_weights.T, slot.T,
        gate_weight[0], up_weight[0], down_weight[0], out_weight,
        gate_b, gate_c, values_u, taps,
    )
    return (outs[0][None], outs[1][None], outs[2][None], *outs[3:])


def solution(mesh):
    placed = (
        P("sp", None),
        P("sp", None),
        P(),
        P("sp", None),
        P("sp", None),
        P("sp", None, "tp"),
        P("sp", None, "tp"),
        P("sp", "tp", None),
        P(None, "tp"),
        P("sp", "tp"),
        P("sp", "tp"),
        P("sp", "tp"),
        P(None, "tp"),
    )
    return jax.shard_map(
        on_device,
        mesh=mesh,
        in_specs=placed,
        out_specs=(
            P("sp", None, "tp"),
            P("sp", None, "tp"),
            P("sp", "tp", None),
            P("sp", None),
            P("sp", "tp"),
            P("sp", "tp"),
            P("sp", "tp"),
            P("sp", "tp"),
        ),
        check_vma=False,
    )
```

time: 227 us -> 217 us (0.956)
  Pallas kernels: 169 us -> 200 us
  starting transfers between devices: 16 us -> 0 us
  waiting for transfers between devices: 13.3 us -> 0 us
  other arithmetic: 10.1 us -> 0.88 us
  matrix products: 8.99 us -> 0.19 us
  local copies, waits for them, and re-layouts: 7.89 us -> 13.1 us
    pallas_call x1, Pallas kernels: 169 us -> 200 us  [on_device(): pl.pallas_call(experts_kernel, out_shape=[jax.ShapeDtypeStruct((width, hi...]
    ppermute x2 -> x0, waiting for transfers between devices: 11.8 us -> none  [passed_along(): return lax.ppermute(array, axis, pairs)]
    all_to_all x1 -> x0, starting transfers between devices: 9.24 us -> none  [sum_at_owner(): tiles = lax.all_to_all(cut_along(array, dim, size), axis, 0, 0, tiled=True)]
    dot_general x4 -> x1, matrix products: 8.99 us -> 0.19 us  [on_device(): jnp.dot((first + second).astype(BF16), (order[:, None] < order[None, :])....]
    ppermute x2 -> x0, starting transfers between devices: 6.73 us -> none  [passed_along(): return lax.ppermute(array, axis, pairs)]
    reduce_sum x3 -> x0, other arithmetic: 4.72 us -> none  [the longest x1 2.15 us: on_device(): jnp.mean(scaled * resid_wide, axis=1, keepdims=True)]
    unnamed x31 -> x24, local copies, waits for them, and re-layouts: 7.1 us -> 11.5 us
    convert_element_type x4 -> x0, other arithmetic: 3.97 us -> none  [the longest x1 1.39 us: on_device(): pick = ((slots[None, :] == slot_of[0][:, None]) | (slots[None, :] == slot...]
  transfers between devices with their start and end apart: 3 -> 0, of which waited for: 2 -> 0; matrix products, arithmetic and copies ran while one was open for 7% -> 0% of each run, Pallas kernels for 75% -> 0%
where the time goes in v2:
time: 217 us; the launch traced here: 215 us
  Pallas kernels  200 us (92%)
  local copies, waits for them, and re-layouts  13.1 us (6%)
    pallas_call x1, Pallas kernels, on_device(): pl.pallas_call(experts_kernel, out_shape=[jax.ShapeDtypeStruct((width, hi...  200 us
    unnamed x24, local copies, waits for them, and re-layouts  11.5 us

profile of v2, /device:TPU:1, one launch (start us, length us, event | category | flops | bytes accessed | tf_op | source)
XLA Modules:
  0.0 215.3 jit_solution(15951339181201660418)
XLA Ops:
  0.7 0.8 slice_reduce_fusion.1
  1.4 0.2 select_reduce_fusion.1
  1.7 0.9 fusion.10
  2.5 0.0 copy-start.7
  2.5 0.8 copy.35
  3.4 0.0 copy-done.7
  3.4 200.3 %shard_map.188 = (f32[2048,256]{1,0:T(8,128)}, f32[2048,256]{1,0:T(8,128)}, f32[256,2048]{1,0:T(8,128)}, bf16[384,2048]{1,0:T(8,128)(2,1)}, f32[64,256]{1,0:T(8,...) custom-call(bf16[384,2048]{1,0:T(8,128)(2,1)} %resid.1, ...), custom_call_target="tpu_custom_call" | custom-call | tf_op jit(solution)/shard_map/pallas_call | solution.py:500
  203.7 0.0 copy-start.1
  203.7 3.2 %copy.44 = f32[1,2048,256]{2,1,0:T(8,128)} copy(f32[1,2048,256]{2,1,0:T(8,128)} %bitcast.51) | data formatting | bytes 4194304
  206.9 0.0 copy-done.1
  206.9 0.0 copy-start
  206.9 1.3 copy.45
  208.2 1.0 copy-done
  209.3 0.0 copy-start.2
  209.3 1.3 copy.46
  210.6 0.8 copy-done.2
  211.4 0.0 copy-start.6
  211.4 0.0 copy-start.5
  211.4 0.0 copy-start.4
  211.4 0.0 copy-start.3
  211.5 1.1 copy.47
  212.6 0.0 copy-done.6
  212.6 0.6 copy.48
  213.2 0.0 copy-done.5
  213.2 0.7 copy.49
  213.9 0.0 copy-done.4
  213.9 0.7 copy.50
  214.6 0.0 copy-done.3
  214.6 0.7 copy.51
  (3 shorter events, 0.0 us)
Async XLA Ops:
  2.5 0.8 copy-start.7
  203.7 3.2 %copy-start.1 = (f32[2048,256]{1,0:T(8,128)S(1)}, f32[2048,256]{1,0:T(8,128)}, u32[]{:S(2)}) copy-start(f32[2048,256]{1,0:T(8,128)} %get-tuple-element.17) | copy-start | bytes 6291460
  206.9 2.3 %copy-start = (f32[256,2048]{1,0:T(8,128)S(1)}, f32[256,2048]{1,0:T(8,128)}, u32[]{:S(2)}) copy-start(f32[256,2048]{1,0:T(8,128)} %get-tuple-element.18) | copy-start | bytes 6291460
  209.3 2.2 %copy-start.2 = (bf16[384,2048]{1,0:T(8,128)(2,1)S(1)}, bf16[384,2048]{1,0:T(8,128)(2,1)}, u32[]{:S(2)}) copy-start(bf16[384,2048]{1,0:T(8,128)(2,1)} %get-tuple-element.41) | copy-start | bytes 4718596
  211.4 1.2 copy-start.6
  211.4 1.8 copy-start.5
  211.4 2.5 %copy-start.4 = (bf16[384,256]{1,0:T(8,128)(2,1)S(1)}, bf16[384,256]{1,0:T(8,128)(2,1)}, u32[]{:S(2)}) copy-start(bf16[384,256]{1,0:T(8,128)(2,1)} %get-tuple-element.44) | copy-start | bytes 589828
  211.4 3.1 %copy-start.3 = (bf16[384,256]{1,0:T(8,128)(2,1)S(1)}, bf16[384,256]{1,0:T(8,128)(2,1)}, u32[]{:S(2)}) copy-start(bf16[384,256]{1,0:T(8,128)(2,1)} %get-tuple-element.45) | copy-start | bytes 589828

commit v3 on v2

--- a/solution.py
+++ b/solution.py
@@ -12,7 +12,7 @@
 BF16 = jnp.bfloat16
 F32 = jnp.float32
 SLOTS = 48
-PER_GROUP = 2
+PER_GROUP = 4
 GROUP_ROWS = PER_GROUP * SLOTS
 GROUPS = 32 // PER_GROUP
 
@@ -67,14 +67,18 @@
 
 
 def experts_kernel(
-    resid, cots, gain, slot, weight, slot_col, gate_w, up_w, down_w, out_w,
-    gate_b, gate_c, values, taps,
+    resid, cots, gain, slot, weight, slot_col, gate_b, gate_c, values, taps,
+    gate_far, up_far, down_far, out_far,
+    to_gate, to_up, to_down, to_resid, to_out, to_b, to_c, to_values,
+    gate_w, up_w, down_w, out_w,
     grad_gate, grad_up, grad_down, grad_resid, grad_out, grad_b, grad_c, grad_values,
+    load_sem, store_sem,
     both, part, extra, swapped, back, hidden, dgate, dup, half_out, half_in, half_own,
-    normed, inverse, pick, total, mixed, conv, merged, dconv, staged, gathered,
+    normed, inverse, pick, total, mixed, conv, merged, dconv, staged, inbox, gathered,
     far_send, far_recv, near_send, near_recv, swap_send, swap_recv, back_send, back_recv,
     out_send, out_recv, all_send, all_recv,
     extra_send, extra_recv, half_send, half_recv, later_send, later_recv, sooner_send, sooner_recv,
+    inbox_send, inbox_recv,
 ):
     s, x = lax.axis_index("sp"), lax.axis_index("tp")
     kind = lax.rem(x, 2)
@@ -98,6 +102,22 @@
             barrier, inc=1, device_id={"sp": moved(s, k, 1), "tp": x}, device_id_type=MESH
         )
 
+    loads = [
+        pltpu.make_async_copy(source, target, load_sem.at[i])
+        for i, (source, target) in enumerate(
+            ((gate_far, gate_w), (up_far, up_w), (down_far, down_w), (out_far, out_w))
+        )
+    ]
+    stores = [
+        pltpu.make_async_copy(source, target, store_sem.at[i])
+        for i, (source, target) in enumerate(
+            (
+                (grad_gate, to_gate), (grad_up, to_up), (grad_down, to_down),
+                (grad_resid, to_resid), (grad_out, to_out), (grad_b, to_b),
+                (grad_c, to_c), (grad_values, to_values),
+            )
+        )
+    ]
     each(1, 32, greet)
     for lane in (right, left, across):
         pl.semaphore_signal(barrier, inc=1, device_id={"sp": s, "tp": lane}, device_id_type=MESH)
@@ -154,6 +174,8 @@
         normed[rows, :] = (held * scale * gain[...]).astype(BF16)
         inverse[rows, :] = jnp.broadcast_to(scale, (64, 128))
 
+    for copy in loads:
+        copy.start()
     each(0, tokens // 64, normalize)
 
     def pack(target, rows, first, count, is_cot):
@@ -299,6 +321,8 @@
         @pl.when(g == 0)
         def _():
             other.start()
+            for copy in loads:
+                copy.wait()
             grad_gate[...] = jnp.zeros_like(grad_gate)
             grad_up[...] = jnp.zeros_like(grad_up)
             grad_down[...] = jnp.zeros_like(grad_down)
@@ -344,6 +368,8 @@
     back[block(0), :] = swapped[block(0), :]
     weights(GROUPS // 2 - 1)
     each(1, 32, lambda k: home(k).wait_recv())
+    for copy in stores[:3]:
+        copy.start()
 
     def summed(half, j):
         return dot_nn(pick[...], back[:, wide(half * 2 + j, 256)])
@@ -396,22 +422,39 @@
         ).astype(BF16)
 
     each(0, tokens // 64, resid_tile)
+    share_rows = grad_out.shape[0]
+    core, chip = lax.rem(s, 2), s // 2
     for j in range(4):
         cols = pl.ds(j * 512, 512)
-        staged[cols, :] = dot_tn(grad_resid[:, cols], merged[...]).astype(BF16)
-    share_rows = grad_out.shape[0]
+        piece = dot_tn(grad_resid[:, cols], merged[...]).astype(BF16)
+        for i in range(8):
+            staged[i % 2, pl.ds((j * 4 + i // 2) * share_rows, share_rows), :] = piece[
+                i * share_rows : (i + 1) * share_rows
+            ]
+    both_cores = remote(
+        staged.at[1 - core], inbox, inbox_send, inbox_recv, moved(s, PARTNER, 1), x
+    )
+
+    def chip_away(k):
+        m = 7 * k
+        z, y = chip // 4, lax.rem(chip, 4)
+        return lax.rem(z + (m // 4) % 4, 4) * 4 + lax.rem(y + m % 4, 4)
 
     def give(k):
-        owner = moved(s, k, 1)
+        owner = chip_away(k)
         return remote(
-            staged.at[wide(owner, share_rows)], gathered.at[k], out_send.at[k], out_recv.at[k],
-            owner, x,
-        )
-
+            staged.at[core, wide(owner, share_rows)], gathered.at[k],
+            out_send.at[k], out_recv.at[k], owner * 2 + core, x,
+        )
+
+    stores[3].start()
+    both_cores.start()
     dmerged = dot_nn(grad_resid[...], out_w[...])
     dconv[pl.ds(0, tokens), :] = dmerged * gate_b[...].astype(F32)
     grad_b[...] = (dmerged * conv[...]).astype(BF16)
-    each(1, 32, lambda k: give(k).start())
+    stores[5].start()
+    both_cores.wait_recv()
+    staged[core] = (staged[core].astype(F32) + inbox[...].astype(F32)).astype(BF16)
 
     @pl.when(s > 0)
     def _():
@@ -421,7 +464,8 @@
     def _():
         dconv[pl.ds(tokens, EDGE), :] = jnp.zeros((EDGE, dconv.shape[1]), F32)
 
-    gathered[0] = staged[wide(s, share_rows), :]
+    gathered[0] = staged[core, wide(chip, share_rows), :]
+    each(1, 16, lambda k: give(k).start())
 
     def finish(k):
         home(k).wait_send()
@@ -452,13 +496,60 @@
     )
     grad_c[...] = (dmixed * values[...].astype(F32)).astype(BF16)
     grad_values[...] = (dmixed * gate_c[...].astype(F32)).astype(BF16)
-    each(1, 32, lambda k: give(k).wait_recv())
+    each(1, 16, lambda k: give(k).wait_recv())
+    for n in (6, 7):
+        stores[n].start()
     grad_out[...] = jnp.sum(gathered[...].astype(F32), axis=0)
-    each(1, 32, lambda k: give(k).wait_send())
+    each(1, 16, lambda k: give(k).wait_send())
+    both_cores.wait_send()
+    stores[4].start()
+    for copy in stores:
+        copy.wait()
 
     @pl.when(s > 0)
     def _():
         sooner.wait_send()
+
+
+CUTS = (4, 4, 4, 3, 1, 1, 1, 1)
+
+
+def hand_over_kernel(*refs):
+    n = len(CUTS)
+    sources, targets, held = refs[:n], refs[n : 2 * n], refs[2 * n : 3 * n]
+    in_sem, out_sem = refs[3 * n :]
+    into, out = [], []
+    for i, cuts in enumerate(CUTS):
+        rows = held[i].shape[0] // cuts
+        for j in range(cuts):
+            part = pl.ds(j * rows, rows)
+            at = len(into)
+            into.append(
+                pltpu.make_async_copy(sources[i].at[part], held[i].at[part], in_sem.at[at])
+            )
+            out.append(
+                pltpu.make_async_copy(held[i].at[part], targets[i].at[part], out_sem.at[at])
+            )
+    for copy in into:
+        copy.start()
+    for arriving, leaving in zip(into, out):
+        arriving.wait()
+        leaving.start()
+    for copy in out:
+        copy.wait()
+
+
+def hand_over(arrays):
+    anywhere = pl.BlockSpec(memory_space=pl.ANY)
+    return pl.pallas_call(
+        hand_over_kernel,
+        out_shape=[jax.ShapeDtypeStruct(a.shape, a.dtype) for a in arrays],
+        in_specs=[anywhere] * len(arrays),
+        out_specs=[anywhere] * len(arrays),
+        scratch_shapes=[pltpu.VMEM(a.shape, a.dtype) for a in arrays]
+        + [pltpu.SemaphoreType.DMA((sum(CUTS),))] * 2,
+        compiler_params=pltpu.CompilerParams(vmem_limit_bytes=60 * 2**20),
+    )(*arrays)
 
 
 def on_device(
@@ -497,9 +588,8 @@
     )
     vmem = pl.BlockSpec(memory_space=pltpu.VMEM)
     dma = pltpu.SemaphoreType.DMA
-    outs = pl.pallas_call(
-        experts_kernel,
-        out_shape=[
+    anywhere = pl.BlockSpec(memory_space=pl.ANY)
+    results = [
             jax.ShapeDtypeStruct((width, hidden), F32),
             jax.ShapeDtypeStruct((width, hidden), F32),
             jax.ShapeDtypeStruct((hidden, width), F32),
@@ -508,10 +598,21 @@
             jax.ShapeDtypeStruct((tokens, channels), BF16),
             jax.ShapeDtypeStruct((tokens, channels), BF16),
             jax.ShapeDtypeStruct((tokens, channels), BF16),
-        ],
-        in_specs=[vmem] * 14,
-        out_specs=[vmem] * 8,
+    ]
+    outs = pl.pallas_call(
+        experts_kernel,
+        out_shape=results,
+        in_specs=[vmem] * 10 + [anywhere] * 4,
+        out_specs=[anywhere] * 8,
         scratch_shapes=[
+            pltpu.VMEM((width, hidden), BF16),
+            pltpu.VMEM((width, hidden), BF16),
+            pltpu.VMEM((hidden, width), BF16),
+            pltpu.VMEM((width, channels), BF16),
+        ]
+        + [pltpu.VMEM(r.shape, r.dtype) for r in results]
+        + [dma((4,)), dma((8,))]
+        + [
             pltpu.VMEM((2, slots, width), BF16),
             pltpu.VMEM((slots, width), BF16),
             pltpu.VMEM((SLOTS, width), BF16),
@@ -531,21 +632,24 @@
             pltpu.VMEM((tokens, channels), F32),
             pltpu.VMEM((tokens, channels), BF16),
             pltpu.VMEM((tokens + EDGE, channels), F32),
-            pltpu.VMEM((width, channels), BF16),
-            pltpu.VMEM((experts, width // experts, channels), BF16),
+            pltpu.VMEM((2, width // 2, channels), BF16),
+            pltpu.VMEM((width // 2, channels), BF16),
+            pltpu.VMEM((experts // 2, width // experts, channels), BF16),
         ]
         + [dma((32,)), dma((32,)), dma((2, 32)), dma((2, 32)), dma((2, 32)), dma((2, 32))]
-        + [dma((32,))] * 4
+        + [dma((32,))] * 2
+        + [dma((16,))] * 2
         + [dma((6,))] * 2
-        + [dma] * 8,
+        + [dma] * 10,
         compiler_params=pltpu.CompilerParams(
             collective_id=0, has_side_effects=True, vmem_limit_bytes=63 * 2**20
         ),
     )(
         resid_in, cotangent, norm_gain[None], slot, route_weights.T, slot.T,
+        gate_b, gate_c, values_u, taps,
         gate_weight[0], up_weight[0], down_weight[0], out_weight,
-        gate_b, gate_c, values_u, taps,
-    )
+    )
+    outs = hand_over(outs)
     return (outs[0][None], outs[1][None], outs[2][None], *outs[3:])
 
 

time: 217 us -> 191 us (0.88)
  Pallas kernels: 200 us -> 187 us
  local copies, waits for them, and re-layouts: 13.1 us -> 1.61 us
    pallas_call x1 -> x2, Pallas kernels: 200 us -> 187 us  [the longest x1 181 us: on_device(): pl.pallas_call(experts_kernel, out_shape=results, in_specs=[vmem] * 10 +...]
    unnamed x24 -> x2, local copies, waits for them, and re-layouts: 11.5 us -> 0.01 us
where the time goes in v3:
time: 191 us
  Pallas kernels  187 us (98%)
    pallas_call x1, Pallas kernels, on_device(): pl.pallas_call(experts_kernel, out_shape=results, in_specs=[vmem] * 10 +...  181 us
    pallas_call x1, Pallas kernels, hand_over(): pl.pallas_call(hand_over_kernel, out_shape=[jax.ShapeDtypeStruct(a.shape,...  6.61 us

profile of v3, /device:TPU:1, one launch (start us, length us, event | category | flops | bytes accessed | tf_op | source)
XLA Modules:
  0.0 190.7 jit_solution(13515373678497844815)
XLA Ops:
  0.7 0.8 slice_reduce_fusion.1
  1.4 0.2 select_reduce_fusion.1
  1.7 0.9 fusion.10
  2.5 0.0 copy-start
  2.5 0.8 copy.35
  3.4 0.0 copy-done
  3.4 180.7 %shard_map.188 = (f32[2048,256]{1,0:T(8,128)}, f32[2048,256]{1,0:T(8,128)}, f32[256,2048]{1,0:T(8,128)}, bf16[384,2048]{1,0:T(8,128)(2,1)}, f32[64,256]{1,0:T(8,...) custom-call(bf16[384,2048]{1,0:T(8,128)(2,1)} %resid.1, ...), custom_call_target="tpu_custom_call" | custom-call | tf_op jit(solution)/shard_map/pallas_call | solution.py:602
  184.1 6.6 %shard_map.189 = (f32[2048,256]{1,0:T(8,128)}, f32[2048,256]{1,0:T(8,128)}, f32[256,2048]{1,0:T(8,128)}, bf16[384,2048]{1,0:T(8,128)(2,1)}, f32[64,256]{1,0:T(8,...) custom-call(f32[2048,256]{1,0:T(8,128)} %get-tuple-element.24.refs_0_, ...), custom_call_target="tpu_custom_call" | custom-call | tf_op jit(solution)/shard_map/pallas_call | solution.py:544
  (3 shorter events, 0.0 us)
Async XLA Ops:
  2.5 0.8 copy-start

commit v4 on v3

--- a/solution.py
+++ b/solution.py
@@ -18,7 +18,7 @@
 
 
 def offsets(k):
-    m = 7 * k
+    m = 13 * k
     return (m // 8) % 4, (m // 2) % 4, m % 2
 
 
@@ -34,7 +34,7 @@
     dz = (expert // 8 - s // 8) % 4
     dy = ((expert // 2) % 4 - (s // 2) % 4) % 4
     dc = (expert - s) % 2
-    return (23 * (dz * 8 + dy * 2 + dc)) % 32
+    return (5 * (dz * 8 + dy * 2 + dc)) % 32
 
 
 def dot_nn(a, b):
@@ -61,7 +61,7 @@
     return pl.ds(pl.multiple_of(j * size, size), size)
 
 
-PARTNER = 23
+PARTNER = 5
 EARLY = 5
 EDGE = 8
 
@@ -316,7 +316,7 @@
 
         @pl.when(g < GROUPS)
         def _():
-            each(jnp.maximum(first, EARLY), first + PER_GROUP, pass_on)
+            each(jnp.maximum(first, EARLY), first + PER_GROUP // 2, pass_on)
 
         @pl.when(g == 0)
         def _():
@@ -346,6 +346,14 @@
 
             each(first - PER_GROUP, first, send)
 
+        @pl.when((g >= 2) & (g <= GROUPS + 1))
+        def _():
+            each(jnp.maximum(first - 2 * PER_GROUP, 1), first - PER_GROUP, lambda k: home(k).start())
+
+        @pl.when(g < GROUPS)
+        def _():
+            each(jnp.maximum(first + PER_GROUP // 2, EARLY), first + PER_GROUP, pass_on)
+
         @pl.when((g >= 2) & (g < GROUPS) & (lax.rem(g, 2) == 0))
         def _():
             weights(g // 2 - 1)
@@ -357,10 +365,6 @@
         @pl.when(g == 5)
         def _():
             make_conv()
-
-        @pl.when((g >= 2) & (g <= GROUPS + 1))
-        def _():
-            each(jnp.maximum(first - 2 * PER_GROUP, 1), first - PER_GROUP, lambda k: home(k).start())
 
         return carry
 

time: 191 us -> 189 us (0.990)
  Pallas kernels: 187 us -> 184 us
    pallas_call x1, Pallas kernels: 181 us -> 177 us  [on_device(): pl.pallas_call(experts_kernel, out_shape=results, in_specs=[vmem] * 10 +...]
where the time goes in v4:
time: 189 us; the launch traced here: 187 us
  Pallas kernels  184 us (97%)
    pallas_call x1, Pallas kernels, on_device(): pl.pallas_call(experts_kernel, out_shape=results, in_specs=[vmem] * 10 +...  177 us
    pallas_call x1, Pallas kernels, hand_over(): pl.pallas_call(hand_over_kernel, out_shape=[jax.ShapeDtypeStruct(a.shape,...  6.61 us

profile of v4, /device:TPU:1, one launch (start us, length us, event | category | flops | bytes accessed | tf_op | source)
XLA Modules:
  0.0 187.3 jit_solution(7423610051122361994)
XLA Ops:
  0.7 0.8 slice_reduce_fusion.1
  1.4 0.2 select_reduce_fusion.1
  1.7 0.9 fusion.10
  2.5 0.0 copy-start
  2.5 0.8 copy.35
  3.4 0.0 copy-done
  3.4 177.3 %shard_map.188 = (f32[2048,256]{1,0:T(8,128)}, f32[2048,256]{1,0:T(8,128)}, f32[256,2048]{1,0:T(8,128)}, bf16[384,2048]{1,0:T(8,128)(2,1)}, f32[64,256]{1,0:T(8,...) custom-call(bf16[384,2048]{1,0:T(8,128)(2,1)} %resid.1, ...), custom_call_target="tpu_custom_call" | custom-call | tf_op jit(solution)/shard_map/pallas_call | solution.py:606
  180.7 6.6 %shard_map.189 = (f32[2048,256]{1,0:T(8,128)}, f32[2048,256]{1,0:T(8,128)}, f32[256,2048]{1,0:T(8,128)}, bf16[384,2048]{1,0:T(8,128)(2,1)}, f32[64,256]{1,0:T(8,...) custom-call(f32[2048,256]{1,0:T(8,128)} %get-tuple-element.24.refs_0_, ...), custom_call_target="tpu_custom_call" | custom-call | tf_op jit(solution)/shard_map/pallas_call | solution.py:548
  (3 shorter events, 0.0 us)
Async XLA Ops:
  2.5 0.8 copy-start
